TPU v7x, 32 devices: a whole 2x2x4 slice. The times are simulated.
32 devices in a mesh: grp: 2 (over y), kv: 4 (over z), tp: 4 (over x, core).
Axes of the slice: x: 2, y: 2, z: 4, core: 2. Of those that a mesh axis runs over, the one named last changes fastest.
Arguments:
- candidate_embeddings: bfloat16 [1536, 4096], P(('grp', 'kv'), 'tp'), parts along dimension 0, may hold values from -100 to 100
- incoming_rms_scaling: float32 [4096], replicated, may hold values from 0.1 to 1.9
- probe_projector: bfloat16 [4096, 2048], P('kv', 'tp'), may hold values from -0.09375 to 0.09375
- address_projector: bfloat16 [4096, 2048], P('kv', 'tp'), may hold values from -0.09375 to 0.09375
- content_projector: bfloat16 [4096, 2048], P('kv', 'tp'), may hold values from -0.09375 to 0.09375
- sigmoid_mask_matrix: bfloat16 [4096, 2048], P('kv', 'tp'), may hold values from -0.09375 to 0.09375
- forgetting_projector: bfloat16 [4096, 16], replicated, may hold values from -0.09375 to 0.09375
- strength_projector_matrix: bfloat16 [4096, 16], replicated, may hold values from -0.09375 to 0.09375
- channel_forgetting_rates: float32 [16], P('tp'), may hold values from -3 to 0.5
- forgetting_offset: float32 [16], P('tp'), may hold values from -1 to 1
- extra_forgetting: float32 [384, 4, 16], P(('grp', 'kv'), None, 'tp'), parts along dimension 0, may hold values from -0.7 to 0, as said below
- outgoing_rms_scaling: float32 [128], replicated, may hold values from 0.1 to 1.9
- final_projector: bfloat16 [2048, 4096], P('tp', 'kv'), may hold values from -0.125 to 0.125
- memory_matrix: float32 [384, 16, 128, 128], P(('grp', 'kv'), 'tp'), parts along dimension 0, may hold values from -4 to 4
- earlier_addresses: bfloat16 [384, 4, 16, 128], P(('grp', 'kv'), None, 'tp'), parts along dimension 0, may hold values from -6 to 6
- earlier_contents: bfloat16 [384, 4, 16, 128], P(('grp', 'kv'), None, 'tp'), parts along dimension 0, may hold values from -6 to 6
- earlier_strengths: float32 [384, 4, 16], P(('grp', 'kv'), None, 'tp'), parts along dimension 0, may hold values from 0.1 to 0.9
- earlier_forgetting: float32 [384, 4, 16], P(('grp', 'kv'), None, 'tp'), parts along dimension 0, may hold values from -1.5 to -0.02
- admitted_counts: int32 [384], P(('grp', 'kv')), parts along dimension 0, may hold values from 0 to 4
Outputs:
- mixed: bfloat16 [1536, 4096], P(('grp', 'kv'), 'tp'), parts along dimension 0
- taken_state: float32 [384, 16, 128, 128], P(('grp', 'kv'), 'tp'), parts along dimension 0
There are 2 independent parts, one for each index of `grp`. A program takes and returns all parts, laid end to end along the dimension named above; an argument that names none is the same for every part. Nothing has to cross between parts.
Inputs may be any that keep to these rules, and one draw needn't show every extreme that they name: `extra_forgetting`: mostly zero; elsewhere the logarithm of a factor between 0.5 and 0.8.
All inputs are finite; a program needn't handle non-finite values.
Results may differ from a plain program's by a relative error of at most 0.015.
Values may be sent and summed in bfloat16 or wider, within the bound.
A program may use at most 128 MiB of HBM per device.

v0:
```python
import jax
import jax.numpy as jnp
from jax import lax
from jax.sharding import PartitionSpec as P

D = 4096
DK = 128
P_SIZE = 4


epsilon = 1e-06
highest = lax.Precision.HIGHEST


def unit_norm(vector):
    return vector * lax.rsqrt(jnp.sum(vector * vector, axis=-1, keepdims=True) + epsilon)


def update(carry, key_vec, value_vec, beta, log_decay):
    decayed = jnp.exp(log_decay)[..., None, None] * carry
    recalled = jnp.einsum("shde,shd->she", decayed, key_vec, precision=highest)
    return decayed + jnp.einsum(
        "shd,she->shde", key_vec, beta[..., None] * (value_vec - recalled), precision=highest
    )


def stored(values):
    return lax.optimization_barrier(values.astype(jnp.bfloat16)).astype(jnp.float32)


def on_device(
    candidate_embeddings,
    incoming_rms_scaling,
    probe_projector,
    address_projector,
    content_projector,
    sigmoid_mask_matrix,
    forgetting_projector,
    strength_projector_matrix,
    channel_forgetting_rates,
    forgetting_offset,
    extra_forgetting,
    outgoing_rms_scaling,
    final_projector,
    memory_matrix,
    earlier_addresses,
    earlier_contents,
    earlier_strengths,
    earlier_forgetting,
    admitted_counts,
):
    rows, local_cols = candidate_embeddings.shape
    width = probe_projector.shape[1]
    heads = width // DK
    seqs_here = rows // P_SIZE
    head_start = lax.axis_index("tp") * heads
    floated = candidate_embeddings.astype(jnp.float32)
    squares = lax.psum(jnp.sum(floated * floated, axis=1), "tp")
    gain_part = lax.dynamic_slice_in_dim(
        incoming_rms_scaling, lax.axis_index("tp") * local_cols, local_cols
    )
    normed_part = (floated * lax.rsqrt(squares / D + epsilon)[:, None] * gain_part).astype(
        jnp.bfloat16
    )
    normed = lax.all_gather(normed_part, "tp", axis=1, tiled=True)
    every = lax.all_to_all(normed, "kv", split_axis=1, concat_axis=0, tiled=True)
    joined = jnp.concatenate(
        [probe_projector, address_projector, content_projector, sigmoid_mask_matrix], axis=1
    )
    summed = lax.psum_scatter(
        jnp.dot(every, joined, preferred_element_type=jnp.float32),
        "kv",
        scatter_dimension=0,
        tiled=True,
    )
    query, keyed, valued, gated = jnp.split(summed, 4, axis=1)

    def shaped(values):
        return stored(values).reshape(seqs_here, P_SIZE, heads, DK)

    query = unit_norm(shaped(query)) * DK ** (-0.5)
    keyed = unit_norm(shaped(keyed))
    valued = shaped(valued)
    gated = shaped(gated)
    decay_cols = lax.dynamic_slice_in_dim(forgetting_projector, head_start, heads, 1)
    beta_cols = lax.dynamic_slice_in_dim(strength_projector_matrix, head_start, heads, 1)
    forgetting_argument = jnp.dot(normed, decay_cols, preferred_element_type=jnp.float32).reshape(
        seqs_here, P_SIZE, heads
    )
    beta_in = jnp.dot(normed, beta_cols, preferred_element_type=jnp.float32).reshape(
        seqs_here, P_SIZE, heads
    )
    forgetting_multiplier = (
        -jnp.exp(channel_forgetting_rates)
        * jax.nn.softplus(forgetting_argument + forgetting_offset)
        + extra_forgetting
    )
    beta = jax.nn.sigmoid(beta_in)
    carried = memory_matrix
    for proposal in range(P_SIZE):
        fresh = update(
            carried,
            unit_norm(earlier_addresses[:, proposal].astype(jnp.float32)),
            earlier_contents[:, proposal].astype(jnp.float32),
            earlier_strengths[:, proposal],
            earlier_forgetting[:, proposal],
        )
        live = (admitted_counts > proposal)[:, None, None, None]
        carried = jnp.where(live, fresh, carried)
    running = carried
    outputs = []
    for proposal in range(P_SIZE):
        running = update(
            running,
            keyed[:, proposal],
            valued[:, proposal],
            beta[:, proposal],
            forgetting_multiplier[:, proposal],
        )
        outputs.append(jnp.einsum("shde,shd->she", running, query[:, proposal], precision=highest))
    attended = jnp.stack(outputs, axis=1)
    scaled = (
        attended
        * lax.rsqrt(jnp.mean(attended * attended, axis=-1, keepdims=True) + epsilon)
        * outgoing_rms_scaling
        * jax.nn.silu(gated)
    )
    flat = scaled.astype(jnp.bfloat16).reshape(rows, width)
    terms = stored(
        jnp.dot(
            flat,
            lax.all_gather(final_projector, "kv", axis=1, tiled=True),
            preferred_element_type=jnp.float32,
        )
    )
    mixed = lax.psum_scatter(terms.astype(jnp.bfloat16), "tp", scatter_dimension=1, tiled=True)
    return (mixed, carried)


def solution(mesh):
    in_specs = (
        P(("grp", "kv"), "tp"),
        P(),
        P("kv", "tp"),
        P("kv", "tp"),
        P("kv", "tp"),
        P("kv", "tp"),
        P(),
        P(),
        P("tp"),
        P("tp"),
        P(("grp", "kv"), None, "tp"),
        P(),
        P("tp", "kv"),
        P(("grp", "kv"), "tp", None, None),
        P(("grp", "kv"), None, "tp", None),
        P(("grp", "kv"), None, "tp", None),
        P(("grp", "kv"), None, "tp"),
        P(("grp", "kv"), None, "tp"),
        P(("grp", "kv")),
    )
    out_specs = (P(("grp", "kv"), "tp"), P(("grp", "kv"), "tp", None, None))
    return jax.shard_map(
        on_device, mesh=mesh, in_specs=in_specs, out_specs=out_specs, check_vma=False
    )
```

profile of v0, /device:TPU:10, one launch (start us, length us, event | category | flops | bytes accessed | tf_op | source)
XLA Modules:
  0.0 399.3 jit_solution(2243327600681373915)
XLA Ops:
  7.2 1.2 fusion.67
  8.4 5.9 %psum.7 = f32[192]{0:T(256)S(1)} all-reduce(f32[192]{0:T(256)S(1)} %fusion.67), channel_id=1, replica_groups=mesh['grp'=2,'kv'=4,'tp'=4] {'tp'}, use_global_device_ids=true, to_apply=%region_1.0 | all-reduce | flops 192 | bytes 1536 | tf_op jit(solution)/shard_map/psum | solution.py:58
  14.3 0.7 dynamic_slice.9
  15.0 1.9 fusion.69
  17.0 20.0 %all-gather.3.cloned.1.call-done = bf16[192,4096]{1,0:T(8,128)(2,1)} async-done(((bf16[192,1024]{1,0:T(8,128)(2,1)}), bf16[192,4096]{1,0:T(8,128)(2,1)}) %all-gather.3.cloned.1.call-update) | async-done | bytes 1572880 | tf_op jit(solution)/shard_map/all_gather | solution.py:65
  37.0 1.5 copy.130
  38.5 40.5 %all_to_all.19 = bf16[192,4,1024]{2,0,1:T(8,128)(2,1)S(1)} all-to-all(bf16[192,4,1024]{2,0,1:T(8,128)(2,1)S(1)} %bitcast.196), channel_id=1, replica_groups=mesh['grp'=2,'kv'=4,'tp'=4] {'kv'}, dimensions={1} | all-to-all | bytes 3145728 | tf_op jit(solution)/shard_map/all_to_all | solution.py:66
  79.1 8.3 %fusion.56 = f32[768,2048]{1,0:T(8,128)} fusion(bf16[768,1024]{1,0:T(8,128)(2,1)S(1)} %bitcast.197, bf16[1024,512]{1,0:T(8,128)(2,1)} %param.24, bf16[1024,512]{1,0:T(8,128)(2,1)} %param.23, bf16[1024,512]{1,0:T(8,128)(2,1)} %param.22, bf16[1024,512]{1,0:T(8,128)(2,1)} %param.21), kind=kOutput, calls=%fused_computation.64 | convolution fusion | flops 3238002688 | bytes 12058624 | tf_op jit(solution)/shard_map/dot_general | solution.py:71
  87.4 0.7 all-gather.5.cloned.1.call-update
  88.1 0.6 reduce-scatter.5.cloned.1.call-start
  89.7 0.3 fusion.78
  90.0 0.3 convert_multiply_fusion.9
  90.3 14.6 %fusion.18 = f32[48,4,1,128]{3,2,1,0:T(1,128)S(1)} fusion(f32[48,4,128,1]{2,3,1,0:T(1,128)S(1)} %bitcast.198, f32[48,4,128,128]{3,2,1,0:T(8,128)} %param.32, f32[48,4]{1,0:T(8,128)S(1)} %copy.78), kind=kOutput, calls=%fused_computation.25 | convolution fusion | flops 40894464 | bytes 12780288 | tf_op jit(solution)/shard_map/shde,shd->she/dot_general | solution.py:21
  105.0 15.6 %fusion.16 = f32[48,4,1,128]{3,2,1,0:T(1,128)S(1)} fusion(f32[48,4,128,1]{2,3,1,0:T(1,128)S(1)} %bitcast.206, f32[48,4,128,128]{3,2,1,0:T(8,128)} %param.32, f32[48,4,128]{2,1,0:T(4,128)S(1)} %fusion.95, f32[48,4,128]{2,1,0:T(4,128)S(1)} %get-tuple-element.22, f32[48,4]{1,0:T(8,128)S(1)} %copy.78, f32[48,4]{1,0:T(8,128)S(1)} %copy.77, ...), kind=kOutput, calls=%fused_computation.23 | convolution fusion | flops 53477376 | bytes 12977712 | tf_op jit(solution)/shard_map/shde,shd->she/dot_general | solution.py:21
  120.8 20.3 %fusion.14 = f32[48,4,1,128]{3,2,1,0:T(1,128)S(1)} fusion(f32[48,4,128,1]{2,3,1,0:T(1,128)S(1)} %bitcast.207, f32[48,4]{1,0:T(8,128)S(1)} %copy.76, f32[48,4,128,128]{3,2,1,0:T(8,128)S(1)} %bitcast.194, f32[48,4,128]{2,1,0:T(4,128)S(1)} %fusion.94, f32[48,4,128]{2,1,0:T(4,128)S(1)} %get-tuple-element.24, f32[48,4,128]{2,1,0:T(4,128)S(1)} %fusion.95, ...), kind=kOutput, calls=%fused_computation.21 | convolution fusion | flops 66060288 | bytes 13175136 | tf_op jit(solution)/shard_map/shde,shd->she/dot_general | solution.py:21
  141.3 23.7 %fusion.12 = f32[48,4,1,128]{3,2,1,0:T(1,128)S(1)} fusion(f32[48,4,128,1]{2,3,1,0:T(1,128)S(1)} %bitcast.205, f32[48,4,128]{2,1,0:T(4,128)S(1)} %fusion.93, f32[48,4,128]{2,1,0:T(4,128)S(1)} %get-tuple-element.25, f32[48,4]{1,0:T(8,128)S(1)} %copy.76, f32[48,4]{1,0:T(8,128)S(1)} %copy.75, pred[48]{0:T(512)(128)(4,1)S(1)} %get-tuple-element.43, ...), kind=kOutput, calls=%fused_computation.19 | convolution fusion | flops 78643200 | bytes 13372560 | tf_op jit(solution)/shard_map/shde,shd->she/dot_general | solution.py:21
  165.2 18.1 %add_select_fusion = f32[48,4,128,128]{3,2,1,0:T(8,128)} fusion(f32[48,4,128]{2,1,0:T(4,128)S(1)} %fusion.92, f32[48,4,128]{2,1,0:T(4,128)S(1)} %get-tuple-element.23, f32[48,4,128]{2,1,0:T(4,128)S(1)} %fusion.93, f32[48,4,128]{2,1,0:T(4,128)S(1)} %get-tuple-element.25, f32[48,4]{1,0:T(8,128)S(1)} %copy.76, f32[48,4]{1,0:T(8,128)S(1)} %copy.75, ...), kind=kLoop, calls=%fused_computation.6 | loop fusion | flops 50331648 | bytes 25955520 | tf_op jit(solution)/shard_map/jit(_where)/select_n | solution.py:109
  183.3 0.5 fusion.97
  183.9 1.4 fusion.66
  185.4 0.1 fusion.106
  185.6 0.4 copy.122
  186.0 0.4 copy.120
  186.4 0.4 copy.118
  186.8 0.4 copy.116
  187.2 0.1 fusion.83
  187.3 0.1 slice_exponential_fusion.3
  187.5 0.4 copy.115
  187.9 0.4 copy.121
  188.3 0.4 copy.119
  188.6 0.4 copy.117
  189.0 9.6 %reduce-scatter.3.cloned.1.call-done = f32[192,2048]{1,0:T(8,128)} async-done(((f32[768,2048]{1,0:T(8,128)}), f32[192,2048]{1,0:T(8,128)}) %reduce-scatter.3.cloned.1.call-update) | async-done | bytes 1572880 | tf_op jit(solution)/shard_map/reduce_scatter | solution.py:70
  198.7 1.5 convert.17
  200.6 0.4 multiply_reduce_fusion.2
  201.0 0.3 broadcast_multiply_fusion.1
  201.4 14.5 %fusion.10 = f32[48,4,1,128]{3,2,1,0:T(1,128)S(1)} fusion(f32[48,4,128,1]{2,3,1,0:T(1,128)S(1)} %bitcast.201, f32[48,4,128,128]{3,2,1,0:T(8,128)} %add_select_fusion, f32[48,4]{1,0:T(8,128)S(1)} %bitcast.215), kind=kOutput, calls=%fused_computation.17 | convolution fusion | flops 40894464 | bytes 12780288 | tf_op jit(solution)/shard_map/shde,shd->she/dot_general | solution.py:21
  216.1 15.1 %fusion.8 = f32[48,4,1,128]{3,2,1,0:T(1,128)S(1)} fusion(f32[48,4,128,1]{2,3,1,0:T(1,128)S(1)} %bitcast.226, f32[48,4,128,128]{3,2,1,0:T(8,128)} %add_select_fusion, f32[48,4]{1,0:T(8,128)S(1)} %bitcast.245, f32[48,4,128]{2,1,0:T(4,128)S(1)} %fusion.91, f32[48,4,128]{2,1,0:T(4,128)S(1)} %get-tuple-element.15, f32[48,4]{1,0:T(8,128)S(1)} %bitcast.216), kind=kOutput, calls=%fused_computation.15 | convolution fusion | flops 50331648 | bytes 12977664 | tf_op jit(solution)/shard_map/shde,shd->she/dot_general | solution.py:21
  231.4 18.4 %fusion.6 = f32[48,4,1,128]{3,2,1,0:T(1,128)S(1)} fusion(f32[48,4,128,1]{2,3,1,0:T(1,128)S(1)} %bitcast.225, f32[48,4]{1,0:T(8,128)S(1)} %bitcast.241, f32[48,4,128,128]{3,2,1,0:T(8,128)S(1)} %bitcast.192, f32[48,4,128]{2,1,0:T(4,128)S(1)} %fusion.89, f32[48,4,128]{2,1,0:T(4,128)S(1)} %get-tuple-element.16, f32[48,4]{1,0:T(8,128)S(1)} %bitcast.246, ...), kind=kOutput, calls=%fused_computation.13 | convolution fusion | flops 59768832 | bytes 13175040 | tf_op jit(solution)/shard_map/shde,shd->she/dot_general | solution.py:21
  250.0 25.3 %fusion.4 = f32[48,4,1,128]{3,2,1,0:T(1,128)S(1)} fusion(f32[48,4,128,1]{2,3,1,0:T(1,128)S(1)} %bitcast.223, f32[48,4]{1,0:T(8,128)S(1)} %bitcast.239, f32[48,4,128]{2,1,0:T(4,128)S(1)} %fusion.87, f32[48,4,128]{2,1,0:T(4,128)S(1)} %get-tuple-element.17, f32[48,4]{1,0:T(8,128)S(1)} %bitcast.242, f32[48,4,128,128]{3,2,1,0:T(8,128)S(1)} %bitcast.192, ...), kind=kOutput, calls=%fused_computation.11 | convolution fusion | flops 69206016 | bytes 13372416 | tf_op jit(solution)/shard_map/shde,shd->she/dot_general | solution.py:21
  275.2 0.4 multiply_reduce_fusion.1
  275.7 0.3 multiply_multiply_fusion
  276.1 12.2 %fusion.20 = f32[48,4,1,128]{3,2,1,0:T(1,128)S(1)} fusion(f32[48,4,128,1]{2,3,1,0:T(1,128)S(1)} %bitcast.202, f32[48,4,128,128]{3,2,1,0:T(8,128)S(1)} %bitcast.192, f32[48,4,128]{2,1,0:T(4,128)S(1)} %fusion.91, f32[48,4,128]{2,1,0:T(4,128)S(1)} %get-tuple-element.15, f32[48,4]{1,0:T(8,128)S(1)} %bitcast.219), kind=kOutput, calls=%fused_computation.27 | convolution fusion | flops 47185920 | bytes 12976896 | tf_op jit(solution)/shard_map/shde,shd->she/dot_general | solution.py:120
  288.3 18.2 %fusion.103 = f32[48,4,1,128]{3,2,1,0:T(1,128)S(1)} fusion(f32[48,4,128,1]{2,3,1,0:T(1,128)S(1)} %bitcast.228, f32[48,4,128,128]{3,2,1,0:T(8,128)S(1)} %bitcast.192, f32[48,4,128]{2,1,0:T(4,128)S(1)} %fusion.89, f32[48,4,128]{2,1,0:T(4,128)S(1)} %get-tuple-element.16, f32[48,4]{1,0:T(8,128)S(1)} %bitcast.248, f32[48,4,128]{2,1,0:T(4,128)S(1)} %fusion.91, ...), kind=kOutput, calls=%fused_computation.171 | convolution fusion | flops 56623104 | bytes 13174272 | tf_op jit(solution)/shard_map/shde,shd->she/dot_general | solution.py:120
  306.5 24.8 %fusion.21 = f32[48,4,1,128]{3,2,1,0:T(1,128)S(1)} fusion(f32[48,4,128,1]{2,3,1,0:T(1,128)S(1)} %bitcast.227, f32[48,4,128]{2,1,0:T(4,128)S(1)} %fusion.87, f32[48,4,128]{2,1,0:T(4,128)S(1)} %get-tuple-element.17, f32[48,4]{1,0:T(8,128)S(1)} %bitcast.243, f32[48,4,128,128]{3,2,1,0:T(8,128)S(1)} %bitcast.192, f32[48,4,128]{2,1,0:T(4,128)S(1)} %fusion.89, ...), kind=kOutput, calls=%fused_computation.28 | convolution fusion | flops 66060288 | bytes 13371648 | tf_op jit(solution)/shard_map/shde,shd->she/dot_general | solution.py:120
  331.3 28.3 %fusion = f32[48,4,1,128]{3,2,1,0:T(1,128)S(1)} fusion(f32[48,4,128,1]{2,3,1,0:T(1,128)S(1)} %bitcast.224, f32[48,4,128]{2,1,0:T(4,128)S(1)} %fusion.85, f32[48,4,128]{2,1,0:T(4,128)S(1)} %get-tuple-element.14, f32[48,4]{1,0:T(8,128)S(1)} %bitcast.240, f32[48,4,128]{2,1,0:T(4,128)S(1)} %fusion.87, f32[48,4,128]{2,1,0:T(4,128)S(1)} %get-tuple-element.17, ...), kind=kOutput, calls=%fused_computation | convolution fusion | flops 75497472 | bytes 13569024 | tf_op jit(solution)/shard_map/shde,shd->she/dot_general | solution.py:120
  359.6 0.4 multiply_reduce_fusion
  360.0 0.3 broadcast_multiply_fusion
  360.3 4.4 %convolution_convert_fusion = bf16[192,4096]{1,0:T(8,128)(2,1)} fusion(bf16[512,4096]{1,0:T(8,128)(2,1)} %all-gather.5.cloned.1.call-done, bf16[192,512]{1,0:T(8,128)(2,1)S(1)} %get-tuple-element.7, f32[24,8,4,128]{3,2,1,0:T(4,128)S(1)} %bitcast.208, f32[512]{0:T(512)S(1)} %broadcast_bitcast_fusion), kind=kOutput, calls=%fused_computation.63 | convolution fusion | flops 806879232 | bytes 6359040 | tf_op jit(solution)/shard_map/dot_general | solution.py:130
  364.7 27.8 %reduce-scatter.5.cloned.1.call-done = bf16[192,1024]{1,0:T(8,128)(2,1)} async-done(((bf16[192,4096]{1,0:T(8,128)(2,1)}), bf16[192,1024]{1,0:T(8,128)(2,1)}) %reduce-scatter.5.cloned.1.call-update) | async-done | bytes 393232 | tf_op jit(solution)/shard_map/reduce_scatter | solution.py:136
  (79 shorter events, 3.1 us)
Async XLA Ops:
  7.2 176.1 %copy-start = (bf16[4096,16]{0,1:T(8,128)(2,1)S(1)}, bf16[4096,16]{0,1:T(8,128)(2,1)}, u32[]{:S(2)}) copy-start(bf16[4096,16]{0,1:T(8,128)(2,1)} %param.25) | copy-start | bytes 393220
  7.2 29.8 %all-gather.3.cloned.1.call-start = ((), (), s32[]{:S(2)}) async-start(), calls=%async_computation.3 | async-start | bytes 1966080 | tf_op jit(solution)/shard_map/all_gather | solution.py:65
  16.9 181.7 %reduce-scatter.3.cloned.1.call-start = ((), (), s32[]{:S(2)}) async-start(), calls=%async_computation.4 | async-start | bytes 7864320 | tf_op jit(solution)/shard_map/reduce_scatter | solution.py:70
  79.0 9.7 %copy-start.10 = (f32[4]{0:T(128)S(1)}, f32[4]{0:T(128)}, u32[]{:S(2)}) copy-start(f32[4]{0:T(128)} %param.27) | copy-start | bytes 52
  79.0 9.7 %copy-start.8 = (f32[128]{0:T(128)S(1)}, f32[128]{0:T(128)}, u32[]{:S(2)}) copy-start(f32[128]{0:T(128)} %param.30) | copy-start | bytes 1540
  79.0 9.7 %copy-start.9 = (s32[48]{0:T(128)S(1)}, s32[48]{0:T(128)}, u32[]{:S(2)}) copy-start(s32[48]{0:T(128)} %param.37) | copy-start | bytes 580
  79.0 9.8 %copy-start.4 = (f32[48,4,4]{0,2,1:T(4,128)S(1)}, f32[48,4,4]{0,2,1:T(4,128)}, u32[]{:S(2)}) copy-start(f32[48,4,4]{0,2,1:T(4,128)} %param.35) | copy-start | bytes 9220
  79.0 9.8 %copy-start.5 = (f32[48,4,4]{0,2,1:T(4,128)S(1)}, f32[48,4,4]{0,2,1:T(4,128)}, u32[]{:S(2)}) copy-start(f32[48,4,4]{0,2,1:T(4,128)} %param.36) | copy-start | bytes 9220
  79.0 10.5 %copy-start.6 = (f32[48,4,4]{0,2,1:T(4,128)S(1)}, f32[48,4,4]{0,2,1:T(4,128)}, u32[]{:S(2)}) copy-start(f32[48,4,4]{0,2,1:T(4,128)} %param.29) | copy-start | bytes 9220
  79.0 10.6 %copy-start.2 = (bf16[48,4,4,128]{3,2,1,0:T(4,128)(2,1)S(1)}, bf16[48,4,4,128]{3,2,1,0:T(4,128)(2,1)}, u32[]{:S(2)}) copy-start(bf16[48,4,4,128]{3,2,1,0:T(4,128)(2,1)} %param.33) | copy-start | bytes 589828
  87.4 17.5 %copy-start.3 = (bf16[48,4,4,128]{3,2,1,0:T(4,128)(2,1)S(1)}, bf16[48,4,4,128]{3,2,1,0:T(4,128)(2,1)}, u32[]{:S(2)}) copy-start(bf16[48,4,4,128]{3,2,1,0:T(4,128)(2,1)} %param.34) | copy-start | bytes 589828
  87.4 272.9 %all-gather.5.cloned.1.call-start = ((), (), s32[]{:S(2)}) async-start(), calls=%async_computation.5 | async-start | bytes 5242880 | tf_op jit(solution)/shard_map/all_gather | solution.py:132
  88.1 304.4 %reduce-scatter.5.cloned.1.call-start = ((), (), s32[]{:S(2)}) async-start(), calls=%async_computation.6 | async-start | bytes 1966080 | tf_op jit(solution)/shard_map/reduce_scatter | solution.py:136
  90.3 30.5 %slice-start.3 = ((s8[12582912]{0:T(1024)(128)(4,1)}), s8[4194304]{0:T(1024)(128)(4,1)S(1)}, s32[]{:S(2)}) async-start(s8[12582912]{0:T(1024)(128)(4,1)} %bitcast.193), calls=%async_computation.10 | async-start | bytes 8388608
  90.3 30.5 %slice-start.4 = ((s8[12582912]{0:T(1024)(128)(4,1)}), s8[4194304]{0:T(1024)(128)(4,1)S(1)}, s32[]{:S(2)}) async-start(s8[12582912]{0:T(1024)(128)(4,1)} %bitcast.193), calls=%async_computation.11 | async-start | bytes 8388608
  105.0 15.8 %slice-start.5 = ((s8[12582912]{0:T(1024)(128)(4,1)}), s8[4194304]{0:T(1024)(128)(4,1)S(1)}, s32[]{:S(2)}) async-start(s8[12582912]{0:T(1024)(128)(4,1)} %bitcast.193), calls=%async_computation.12 | async-start | bytes 8388608
  165.1 18.2 %copy-start.1 = (bf16[192,4096]{1,0:T(8,128)(2,1)S(1)}, bf16[192,4096]{1,0:T(8,128)(2,1)}, u32[]{:S(2)}) copy-start(bf16[192,4096]{1,0:T(8,128)(2,1)} %all-gather.3.cloned.1.call-done) | copy-start | bytes 4718596
  165.1 22.0 %copy-start.7 = (f32[4]{0:T(128)S(1)}, f32[4]{0:T(128)}, u32[]{:S(2)}) copy-start(f32[4]{0:T(128)} %param.28) | copy-start | bytes 52
  201.4 29.9 %slice-start = ((s8[12582912]{0:T(1024)(128)(4,1)}), s8[4194304]{0:T(1024)(128)(4,1)S(1)}, s32[]{:S(2)}) async-start(s8[12582912]{0:T(1024)(128)(4,1)} %bitcast.191), calls=%async_computation.7 | async-start | bytes 8388608
  201.4 29.9 %slice-start.1 = ((s8[12582912]{0:T(1024)(128)(4,1)}), s8[4194304]{0:T(1024)(128)(4,1)S(1)}, s32[]{:S(2)}) async-start(s8[12582912]{0:T(1024)(128)(4,1)} %bitcast.191), calls=%async_computation.8 | async-start | bytes 8388608
  216.1 15.3 %slice-start.2 = ((s8[12582912]{0:T(1024)(128)(4,1)}), s8[4194304]{0:T(1024)(128)(4,1)S(1)}, s32[]{:S(2)}) async-start(s8[12582912]{0:T(1024)(128)(4,1)} %bitcast.191), calls=%async_computation.9 | async-start | bytes 8388608
Sparse Core Ops, SparseCore 0:
  17.0 19.9 all-gather.2
  87.5 111.1 reduce-scatter.2
  200.2 78.7 all-gather.4
  364.9 27.5 reduce-scatter.4
where the time goes:
time: 405 us; the launch traced here: 399 us
  matrix products  246 us (61%)
  waiting for transfers between devices  58.2 us (14%)
  blocking collectives  46.4 us (11%)
  other arithmetic  26.4 us (7%)
  between operations  14.6 us (4%)
  local copies, waits for them, and re-layouts  7.47 us (2%)
    dot_general x8, matrix products, update(): recalled = jnp.einsum('shde,shd->she', decayed, key_vec, precision=highest)  148 us
    dot_general x4, matrix products, on_device(): jnp.einsum('shde,shd->she', running, query[:, proposal], precision=highest)  83.5 us
    all_to_all x1, blocking collectives, on_device(): lax.all_to_all(normed, 'kv', split_axis=1, concat_axis=0, tiled=True)  40.5 us
    reduce_scatter x1, waiting for transfers between devices, on_device(): lax.psum_scatter(terms.astype(jnp.bfloat16), 'tp', scatter_dimension=1, t...  27.8 us
    all_gather x1, waiting for transfers between devices, on_device(): normed = lax.all_gather(normed_part, 'tp', axis=1, tiled=True)  20 us
    select_n x1, other arithmetic, on_device(): carried = jnp.where(live, fresh, carried)  18.1 us
    reduce_scatter x1, waiting for transfers between devices, on_device(): lax.psum_scatter(jnp.dot(every, joined, preferred_element_type=jnp.float3...  9.62 us
    dot_general x1, matrix products, on_device(): jnp.dot(every, joined, preferred_element_type=jnp.float32)  8.31 us
  transfers between devices with their start and end apart: 4, of which 3 were waited for; matrix products, arithmetic and copies ran while one was open for 65% of the time, Pallas kernels for 0%

commit v1 on v0

v1 whole, which is shorter than its diff:
```python
import functools

import jax
import jax.numpy as jnp
from jax import lax
from jax.experimental import pallas as pl
from jax.experimental.pallas import tpu as pltpu
from jax.sharding import PartitionSpec as P

DK = 128
P_SIZE = 4
SB = 8
TALL = SB * P_SIZE
epsilon = 1e-06
f32 = jnp.float32
bf16 = jnp.bfloat16


def lane_dot(a, b):
    return jnp.sum(a * b, axis=-1, keepdims=True)


def first_half():
    return lax.broadcasted_iota(jnp.int32, (8, DK), 0) < P_SIZE


def load_heads(heads, src, dst):
    for h in range(heads):
        dst[pl.ds(h * TALL, TALL), :] = src[:, h * DK : (h + 1) * DK].astype(f32)


def tile(h, pair):
    return pl.ds(h * TALL + pair * 8, 8)


def proposal(h, p):
    return pl.ds(h * TALL + p, SB, stride=P_SIZE)


def accepted_kernel(heads, s_ref, k_ref, v_ref, f_ref, b_ref, n_ref, o_ref, r_scr, u_scr, c_scr, kf, vf):
    load_heads(heads, k_ref, kf)
    load_heads(heads, v_ref, vf)
    low = first_half()
    for pair in range(SB // 2):
        for h in range(heads):
            at = tile(h, pair)
            lhs = kf[at, :].astype(bf16)
            r0 = jnp.dot(lhs, s_ref[2 * pair, h].astype(bf16), preferred_element_type=f32)
            r1 = jnp.dot(lhs, s_ref[2 * pair + 1, h].astype(bf16), preferred_element_type=f32)
            r_scr[at, :] = jnp.where(low, r0, r1)
    count = n_ref[...]
    for h in range(heads):
        scale = jnp.ones((SB, 1), f32)
        ks, us, norms = [], [], []
        for p in range(P_SIZE):
            at = proposal(h, p)
            col = slice(p * heads + h, p * heads + h + 1)
            key = kf[at, :]
            norm = lax.rsqrt(lane_dot(key, key) + epsilon)
            live = count > p
            g = jnp.where(live, jnp.exp(f_ref[:, col]), 1.0)
            b = jnp.where(live, b_ref[:, col], 0.0)
            rec = (scale * norm) * r_scr[at, :]
            for ki, ui, ni in zip(ks, us, norms):
                rec = rec + (lane_dot(ki, key) * (ni * norm)) * ui
            us = [ui * g for ui in us]
            scale = scale * g
            us.append(b * (vf[at, :] - g * rec))
            ks.append(key)
            norms.append(norm)
        for p in range(P_SIZE):
            u_scr[proposal(h, p), :] = us[p] * norms[p]
        c_scr[pl.ds(h * SB, SB), :] = jnp.broadcast_to(scale, (SB, DK))
    for pair in range(SB // 2):
        for h in range(heads):
            at = tile(h, pair)
            key = kf[at, :]
            lhs = jnp.concatenate([key, key], axis=0).astype(bf16)
            u = u_scr[at, :]
            hi = u.astype(bf16).astype(f32)
            lo = u - hi
            for half in range(2):
                keep = low if half == 0 else jnp.logical_not(low)
                rhs = jnp.concatenate([jnp.where(keep, hi, 0.0), jnp.where(keep, lo, 0.0)], axis=0).astype(bf16)
                seq = 2 * pair + half
                add = lax.dot_general(lhs, rhs, (((0,), (0,)), ((), ())), preferred_element_type=f32)
                o_ref[seq, h] = c_scr[pl.ds(h * SB + seq, 1), :] * s_ref[seq, h] + add


def attend_kernel(heads, s_ref, q_ref, k_ref, v_ref, z_ref, d_ref, b_ref, w_ref, o_ref, rk, rq, qf, kf, vf, zf, of):
    for src, dst in ((q_ref, qf), (k_ref, kf), (v_ref, vf), (z_ref, zf)):
        load_heads(heads, src, dst)
    low = first_half()
    for pair in range(SB // 2):
        for h in range(heads):
            at = tile(h, pair)
            lhs = jnp.concatenate([kf[at, :], qf[at, :]], axis=0).astype(bf16)
            r0 = jnp.dot(lhs, s_ref[2 * pair, h].astype(bf16), preferred_element_type=f32)
            r1 = jnp.dot(lhs, s_ref[2 * pair + 1, h].astype(bf16), preferred_element_type=f32)
            rk[at, :] = jnp.where(low, r0[:8], r1[:8])
            rq[at, :] = jnp.where(low, r0[8:], r1[8:])
    gain = w_ref[...]
    for h in range(heads):
        scale = jnp.ones((SB, 1), f32)
        ks, us, norms = [], [], []
        for p in range(P_SIZE):
            at = proposal(h, p)
            col = slice(p * heads + h, p * heads + h + 1)
            key = kf[at, :]
            query = qf[at, :]
            norm = lax.rsqrt(lane_dot(key, key) + epsilon)
            qnorm = lax.rsqrt(lane_dot(query, query) + epsilon) * DK ** (-0.5)
            g = jnp.exp(d_ref[:, col])
            rec = (scale * norm) * rk[at, :]
            for ki, ui, ni in zip(ks, us, norms):
                rec = rec + (lane_dot(ki, key) * (ni * norm)) * ui
            us = [ui * g for ui in us]
            scale = scale * g
            us.append(b_ref[:, col] * (vf[at, :] - g * rec))
            ks.append(key)
            norms.append(norm)
            att = (scale * qnorm) * rq[at, :]
            for ki, ui, ni in zip(ks, us, norms):
                att = att + (lane_dot(ki, query) * (ni * qnorm)) * ui
            gate = zf[at, :]
            mean = jnp.sum(att * att, axis=-1, keepdims=True) / DK
            of[at, :] = att * lax.rsqrt(mean + epsilon) * gain * (gate * jax.nn.sigmoid(gate))
    for h in range(heads):
        o_ref[:, h * DK : (h + 1) * DK] = of[pl.ds(h * TALL, TALL), :].astype(bf16)


def accepted(state, keys, values, forgetting, strengths, counts):
    seqs, heads = state.shape[:2]
    width = heads * DK
    rows = TALL
    tall = pl.BlockSpec((rows, width), lambda i: (i, 0))
    thin = pl.BlockSpec((SB, P_SIZE * heads), lambda i: (i, 0))
    block = pl.BlockSpec((SB, heads, DK, DK), lambda i: (i, 0, 0, 0))
    return pl.pallas_call(
        functools.partial(accepted_kernel, heads),
        grid=(seqs // SB,),
        in_specs=[block, tall, tall, thin, thin, pl.BlockSpec((SB, 1), lambda i: (i, 0))],
        out_specs=block,
        out_shape=jax.ShapeDtypeStruct(state.shape, f32),
        scratch_shapes=[pltpu.VMEM((heads * n, DK), f32) for n in (TALL, TALL, SB, TALL, TALL)],
        cost_estimate=pl.CostEstimate(flops=10_000_000_000, bytes_accessed=2 * state.size * 4, transcendentals=0),
        name="accepted",
    )(state, keys, values, forgetting, strengths, counts)


def attend(state, packed, decay, beta, gain):
    seqs, heads = state.shape[:2]
    width = heads * DK
    rows = TALL
    thin = pl.BlockSpec((SB, P_SIZE * heads), lambda i: (i, 0))
    block = pl.BlockSpec((SB, heads, DK, DK), lambda i: (i, 0, 0, 0))

    def part(n):
        return pl.BlockSpec((rows, width), lambda i: (i, n))

    return pl.pallas_call(
        functools.partial(attend_kernel, heads),
        grid=(seqs // SB,),
        in_specs=[block, part(0), part(1), part(2), part(3), thin, thin, pl.BlockSpec((1, DK), lambda i: (0, 0))],
        out_specs=pl.BlockSpec((rows, width), lambda i: (i, 0)),
        out_shape=jax.ShapeDtypeStruct((seqs * P_SIZE, width), bf16),
        scratch_shapes=[pltpu.VMEM((heads * TALL, DK), f32)] * 7,
        cost_estimate=pl.CostEstimate(flops=5_000_000_000, bytes_accessed=state.size * 4, transcendentals=0),
        name="attend",
    )(state, packed, packed, packed, packed, decay, beta, gain.reshape(1, DK))


def on_device(
    n_kv,
    n_tp,
    candidate_embeddings,
    incoming_rms_scaling,
    probe_projector,
    address_projector,
    content_projector,
    sigmoid_mask_matrix,
    forgetting_projector,
    strength_projector_matrix,
    channel_forgetting_rates,
    forgetting_offset,
    extra_forgetting,
    outgoing_rms_scaling,
    final_projector,
    memory_matrix,
    earlier_addresses,
    earlier_contents,
    earlier_strengths,
    earlier_forgetting,
    admitted_counts,
):
    rows, local_cols = candidate_embeddings.shape
    features = incoming_rms_scaling.shape[0]
    depth, width = probe_projector.shape
    heads = width // DK
    seqs = rows // P_SIZE
    square = n_kv == n_tp
    swap = [(a * n_tp + b, b * n_tp + a) for a in range(n_kv) for b in range(n_tp)] if square else None
    k_index, t_index = lax.axis_index("kv"), lax.axis_index("tp")

    def thin(values):
        return values.reshape(seqs, P_SIZE * heads)

    if square:
        turned = lax.ppermute(candidate_embeddings, ("kv", "tp"), swap)
        every = lax.all_gather(turned, "tp", axis=0, tiled=True)
    else:
        every = lax.all_gather(candidate_embeddings, "tp", axis=1, tiled=True)
        every = lax.all_to_all(every, "kv", split_axis=1, concat_axis=0, tiled=True)
    gain_part = lax.dynamic_slice_in_dim(incoming_rms_scaling, k_index * depth, depth)
    floated = every.astype(f32)
    gained = (floated * gain_part).astype(bf16)
    decay_cols = lax.dynamic_slice(forgetting_projector, (k_index * depth, t_index * heads), (depth, heads))
    beta_cols = lax.dynamic_slice(strength_projector_matrix, (k_index * depth, t_index * heads), (depth, heads))
    few = jnp.concatenate(
        [
            jnp.dot(gained, jnp.concatenate([decay_cols, beta_cols], axis=1), preferred_element_type=f32),
            jnp.sum(floated * floated, axis=1, keepdims=True),
        ],
        axis=1,
    )
    few = lax.psum_scatter(few, "kv", scatter_dimension=0, tiled=True)
    partial = jnp.concatenate(
        [
            jnp.dot(gained, w, preferred_element_type=f32).astype(bf16)
            for w in (probe_projector, address_projector, content_projector, sigmoid_mask_matrix)
        ],
        axis=1,
    )
    summed = lax.psum_scatter(partial, "kv", scatter_dimension=0, tiled=True)
    taken = accepted(
        memory_matrix,
        earlier_addresses.reshape(rows, width),
        earlier_contents.reshape(rows, width),
        thin(earlier_forgetting),
        thin(earlier_strengths),
        admitted_counts.reshape(seqs, 1),
    )
    factor = lax.rsqrt(few[:, 2 * heads :] / features + epsilon)
    few = few[:, : 2 * heads] * factor
    packed = (summed.astype(f32) * factor).astype(bf16)
    decay_in = few[:, :heads].reshape(seqs, P_SIZE, heads)
    beta = jax.nn.sigmoid(few[:, heads:].reshape(seqs, P_SIZE, heads))
    decay = -jnp.exp(channel_forgetting_rates) * jax.nn.softplus(decay_in + forgetting_offset) + extra_forgetting
    flat = attend(taken, packed, thin(decay), thin(beta), outgoing_rms_scaling)
    gathered = lax.all_gather(flat, "kv", axis=0, tiled=True)
    terms = jnp.dot(gathered, final_projector, preferred_element_type=f32).astype(bf16)
    if square:
        mixed = lax.psum_scatter(terms, "tp", scatter_dimension=0, tiled=True)
        mixed = lax.ppermute(mixed, ("kv", "tp"), swap)
    else:
        terms = lax.all_to_all(terms, "kv", split_axis=0, concat_axis=1, tiled=True)
        mixed = lax.psum_scatter(terms, "tp", scatter_dimension=1, tiled=True)
    return (mixed, taken)


def solution(mesh):
    row, per_head = P(("grp", "kv"), "tp"), P(("grp", "kv"), None, "tp")
    four = P(("grp", "kv"), None, "tp", None)
    weight = P("kv", "tp")
    state = P(("grp", "kv"), "tp", None, None)
    in_specs = (
        row, P(), weight, weight, weight, weight, P(), P(), P("tp"), P("tp"), per_head, P(),
        P("tp", "kv"), state, four, four, per_head, per_head, P(("grp", "kv")),
    )
    body = functools.partial(on_device, mesh.shape["kv"], mesh.shape["tp"])
    return jax.shard_map(body, mesh=mesh, in_specs=in_specs, out_specs=(row, state), check_vma=False)
```

time: 405 us -> 232 us (0.57); the launches traced: 399 us -> 230 us
  matrix products: 246 us -> 9.32 us
  waiting for transfers between devices: 58.2 us -> 138 us
  blocking collectives: 46.4 us -> 17.4 us
  Pallas kernels: 0 us -> 27 us
  other arithmetic: 26.4 us -> 7.13 us
  starting transfers between devices: 0.68 us -> 6.76 us
    dot_general x16 -> x6, matrix products: 246 us -> 9.32 us  [the longest x4 5.23 us: on_device(): jnp.dot(gained, w, preferred_element_type=f32).astype(bf16)]
    reduce_scatter x2, waiting for transfers between devices: 37.4 us -> 82.5 us  [the longest x1 54.1 us: on_device(): summed = lax.psum_scatter(partial, 'kv', scatter_dimension=0, tiled=True)]
    all_to_all x1 -> x0, blocking collectives: 40.5 us -> none  [on_device(): lax.all_to_all(normed, 'kv', split_axis=1, concat_axis=0, tiled=True)]
    ppermute x0 -> x2, waiting for transfers between devices: none -> 38.5 us  [the longest x1 19.5 us: on_device(): turned = lax.ppermute(candidate_embeddings, ('kv', 'tp'), swap)]
    pallas_call x0 -> x2, Pallas kernels: none -> 27 us  [the longest x1 13.9 us: attend(): pl.pallas_call(functools.partial(attend_kernel, heads), grid=(seqs // SB,...]
    select_n x1 -> x0, other arithmetic: 18.1 us -> none  [on_device(): carried = jnp.where(live, fresh, carried)]
    all_gather x0 -> x1, blocking collectives: none -> 17.4 us  [on_device(): gathered = lax.all_gather(flat, 'kv', axis=0, tiled=True)]
    ppermute x0 -> x2, starting transfers between devices: none -> 6.6 us  [the longest x1 3.57 us: on_device(): mixed = lax.ppermute(mixed, ('kv', 'tp'), swap)]
  transfers between devices with their start and end apart: 4 -> 6, of which waited for: 3 -> 5; matrix products, arithmetic and copies ran while one was open for 65% -> 7% of each run, Pallas kernels for 0% -> 6%
where the time goes in v1:
time: 232 us; the launch traced here: 230 us
  waiting for transfers between devices  138 us (59%)
  Pallas kernels  27 us (12%)
  blocking collectives  17.4 us (7%)
  between operations  14 us (6%)
  local copies, waits for them, and re-layouts  11.4 us (5%)
  matrix products  9.32 us (4%)
  other arithmetic  7.13 us (3%)
  starting transfers between devices  6.76 us (3%)
    reduce_scatter x1, waiting for transfers between devices, on_device(): summed = lax.psum_scatter(partial, 'kv', scatter_dimension=0, tiled=True)  54.1 us
    reduce_scatter x1, waiting for transfers between devices, on_device(): mixed = lax.psum_scatter(terms, 'tp', scatter_dimension=0, tiled=True)  28.4 us
    ppermute x1, waiting for transfers between devices, on_device(): turned = lax.ppermute(candidate_embeddings, ('kv', 'tp'), swap)  19.5 us
    ppermute x1, waiting for transfers between devices, on_device(): mixed = lax.ppermute(mixed, ('kv', 'tp'), swap)  19 us
    all_gather x1, blocking collectives, on_device(): gathered = lax.all_gather(flat, 'kv', axis=0, tiled=True)  17.4 us
    all_gather x1, waiting for transfers between devices, on_device(): every = lax.all_gather(turned, 'tp', axis=0, tiled=True)  16.5 us
    pallas_call x1, Pallas kernels, attend(): pl.pallas_call(functools.partial(attend_kernel, heads), grid=(seqs // SB,...  13.9 us
    pallas_call x1, Pallas kernels, accepted(): pl.pallas_call(functools.partial(accepted_kernel, heads), grid=(seqs // S...  13 us
  transfers between devices with their start and end apart: 6, of which 5 were waited for; matrix products, arithmetic and copies ran while one was open for 7% of the time, Pallas kernels for 6%

profile of v1, /device:TPU:10, one launch (start us, length us, event | category | flops | bytes accessed | tf_op | source)
XLA Modules:
  0.0 230.5 jit_solution(1254044968096428728)
XLA Ops:
  7.2 0.0 all-gather.2.cloned.1.call-start
  7.2 3.0 %collective-permute-start = (bf16[192,1024]{1,0:T(8,128)(2,1)}, bf16[192,1024]{1,0:T(8,128)(2,1)S(1)}, u32[]{:S(2)}, u32[]{:S(2)}) collective-permute-start(bf16[192,1024]{1,0:T(8,128)(2,1)} %param.19), channel_id=1, source_target_pairs={{0,0},{1,4},{2,8},{3,12},{4,1},{5,5},{6,9},{7,13},{8,2},{9,6},{10,... | collective-permute-start | bytes 1179656 | tf_op jit(solution)/shard_map/ppermute | solution.py:209
  10.3 19.5 %collective-permute-done = bf16[192,1024]{1,0:T(8,128)(2,1)S(1)} collective-permute-done((bf16[192,1024]{1,0:T(8,128)(2,1)}, bf16[192,1024]{1,0:T(8,128)(2,1)S(1)}, u32[]{:S(2)}, u32[]{:S(2)}) %collective-permute-start) | collective-permute-done | bytes 393248 | tf_op jit(solution)/shard_map/ppermute | solution.py:209
  29.8 0.7 copy-done.2
  30.5 0.0 all-gather.2.cloned.1.call-update
  30.5 0.0 reduce-scatter.10.cloned.1.call-start
  30.6 0.7 dynamic_slice.9
  31.3 0.8 dynamic_slice.10
  32.1 0.8 dynamic_slice.11
  32.9 16.5 %all-gather.2.cloned.1.call-done = bf16[768,1024]{1,0:T(8,128)(2,1)} async-done(((bf16[192,1024]{1,0:T(8,128)(2,1)}), bf16[768,1024]{1,0:T(8,128)(2,1)}) %all-gather.2.cloned.1.call-update) | async-done | bytes 1572880 | tf_op jit(solution)/shard_map/all_gather | solution.py:210
  49.4 1.9 fusion.1
  51.3 1.9 fusion.2
  53.3 0.9 copy.59
  54.2 0.0 reduce-scatter.10.cloned.1.call-update
  54.2 0.0 reduce-scatter.6.cloned.1.call-start
  54.3 2.3 convolution_convert_fusion.3
  56.6 1.0 convolution_convert_fusion.2
  57.6 0.2 copy-done.11
  57.8 1.0 convolution_convert_fusion.1
  58.8 0.2 copy-done.12
  59.1 1.0 convolution_convert_fusion.4
  60.1 1.9 pad_maximum_fusion
  62.0 0.0 reduce-scatter.6.cloned.1.call-update
  62.0 0.0 reduce-scatter.8.cloned.1.call-start
  62.0 0.6 copy-done.6
  62.6 0.7 copy.46.b_ref
  63.3 0.7 copy.45.f_ref
  64.0 0.7 copy.47.n_ref
  64.7 0.8 copy_bitcast_fusion
  65.5 13.0 %accepted.1.s_ref = f32[48,4,128,128]{3,2,1,0:T(8,128)} custom-call(f32[48,4,128,128]{3,2,1,0:T(8,128)} %s_ref.1, bf16[192,512]{1,0:T(8,128)(2,1)} %get-tuple-element.5.k_ref, bf16[192,512]{1,0:T(8,128)(2,1)} %get-tuple-element.4.v_ref, f32[48,16]{1,0:T(8,128)} %copy.45.f_ref, f32[48,16]{1,0:T(8,128)} %copy.46.b_ref, s32[48,1]{1,0:T(8,128)} %copy.47.n_ref), custom_call_target="tpu_custom_call" | custom-call | flops 10000000000 | bytes 25165824 | tf_op jit(solution)/shard_map/accepted/pallas_call | solution.py:139
  78.6 0.9 copy.62
  79.5 1.0 add_rsqrt_fusion
  80.5 0.1 copy.65
  80.6 0.1 copy.53
  80.8 0.7 div.16.b_ref
  81.5 0.1 reshape.45
  81.6 0.1 copy.52
  81.7 0.1 fusion.12
  81.8 0.7 copy.54.d_ref
  82.5 54.1 %reduce-scatter.6.cloned.1.call-done = bf16[192,2048]{1,0:T(8,128)(2,1)} async-done(((bf16[768,2048]{1,0:T(8,128)(2,1)}), bf16[192,2048]{1,0:T(8,128)(2,1)}) %reduce-scatter.6.cloned.1.call-update) | async-done | bytes 786448 | tf_op jit(solution)/shard_map/reduce_scatter | solution.py:234
  136.5 2.2 multiply_convert_fusion.q_ref.k_ref.v_ref.z_ref
  138.8 13.9 %attend.1 = bf16[192,512]{1,0:T(8,128)(2,1)} custom-call(f32[48,4,128,128]{3,2,1,0:T(8,128)} %accepted.1.s_ref, bf16[192,2048]{1,0:T(8,128)(2,1)} %multiply_convert_fusion.q_ref.k_ref.v_ref.z_ref, bf16[192,2048]{1,0:T(8,128)(2,1)} %multiply_convert_fusion.q_ref.k_ref.v_ref.z_ref, bf16[192,2048]{1,0:T(8,128)(2,1)} %multiply_convert_fusion.q_ref.k_ref.v_ref.z_ref, ...), custom_call_target="tpu_custom_call" | custom-call | flops 5000000000 | bytes 12582912 | tf_op jit(solution)/shard_map/attend/pallas_call | solution.py:161
  152.7 17.4 %all_gather.7 = bf16[768,512]{1,0:T(8,128)(2,1)S(1)} all-gather(bf16[192,512]{1,0:T(8,128)(2,1)} %attend.1), channel_id=1, replica_groups=mesh['grp'=2,'kv'=4,'tp'=4] {'kv'}, dimensions={0}, use_global_device_ids=true | all-gather | bytes 983040 | tf_op jit(solution)/shard_map/all_gather | solution.py:250
  170.0 2.2 convolution_convert_fusion
  172.2 28.4 %reduce-scatter.8.cloned.1.call-done = bf16[192,1024]{1,0:T(8,128)(2,1)} async-done(((bf16[768,1024]{1,0:T(8,128)(2,1)}), bf16[192,1024]{1,0:T(8,128)(2,1)}) %reduce-scatter.8.cloned.1.call-update) | async-done | bytes 393232 | tf_op jit(solution)/shard_map/reduce_scatter | solution.py:253
  200.7 3.6 %collective-permute-start.1 = (bf16[192,1024]{1,0:T(8,128)(2,1)}, bf16[192,1024]{1,0:T(8,128)(2,1)S(1)}, u32[]{:S(2)}, u32[]{:S(2)}) collective-permute-start(bf16[192,1024]{1,0:T(8,128)(2,1)} %reduce-scatter.8.cloned.1.call-done), channel_id=1, source_target_pairs={{0,0},{1,4},{2,8},{3,12},{4,1},{5,5},{6,9},{7,13},{8,2},{9,6},{10,... | collective-permute-start | bytes 1179656 | tf_op jit(solution)/shard_map/ppermute | solution.py:254
  204.2 19.0 %collective-permute-done.1 = bf16[192,1024]{1,0:T(8,128)(2,1)S(1)} collective-permute-done((bf16[192,1024]{1,0:T(8,128)(2,1)}, bf16[192,1024]{1,0:T(8,128)(2,1)S(1)}, u32[]{:S(2)}, u32[]{:S(2)}) %collective-permute-start.1) | collective-permute-done | bytes 393248 | tf_op jit(solution)/shard_map/ppermute | solution.py:254
  223.2 0.7 copy.69
  (31 shorter events, 0.1 us)
Async XLA Ops:
  7.2 162.9 %copy-start = (bf16[512,1024]{1,0:T(8,128)(2,1)S(1)}, bf16[512,1024]{1,0:T(8,128)(2,1)}, u32[]{:S(2)}) copy-start(bf16[512,1024]{1,0:T(8,128)(2,1)} %param.31) | copy-start | bytes 3145732
  7.2 42.2 %all-gather.2.cloned.1.call-start = ((), (), s32[]{:S(2)}) async-start(), calls=%async_computation.3 | async-start | bytes 1966080 | tf_op jit(solution)/shard_map/all_gather | solution.py:210
  7.2 22.5 %collective-permute-start = (bf16[192,1024]{1,0:T(8,128)(2,1)}, bf16[192,1024]{1,0:T(8,128)(2,1)S(1)}, u32[]{:S(2)}, u32[]{:S(2)}) collective-permute-start(bf16[192,1024]{1,0:T(8,128)(2,1)} %param.19), channel_id=1, source_target_pairs={{0,0},{1,4},{2,8},{3,12},{4,1},{5,5},{6,9},{7,13},{8,2},{9,6},{10,... | collective-permute-start | bytes 1179656 | tf_op jit(solution)/shard_map/ppermute | solution.py:209
  29.8 0.7 copy-start.2
  30.5 48.0 %reduce-scatter.10.cloned.1.call-start = ((), (), s32[]{:S(2)}) async-start(), calls=%async_computation.6 | async-start | bytes 491520
  49.4 4.9 %copy-start.1 = (bf16[768,1024]{1,0:T(8,128)(2,1)S(1)}, bf16[768,1024]{1,0:T(8,128)(2,1)}, u32[]{:S(2)}) copy-start(bf16[768,1024]{1,0:T(8,128)(2,1)} %all-gather.2.cloned.1.call-done) | copy-start | bytes 4718596
  54.2 82.3 %reduce-scatter.6.cloned.1.call-start = ((), (), s32[]{:S(2)}) async-start(), calls=%async_computation.4 | async-start | bytes 3932160 | tf_op jit(solution)/shard_map/reduce_scatter | solution.py:234
  54.3 2.3 %copy-start.10 = (bf16[1024,512]{1,0:T(8,128)(2,1)S(1)}, bf16[1024,512]{1,0:T(8,128)(2,1)}, u32[]{:S(2)}) copy-start(bf16[1024,512]{1,0:T(8,128)(2,1)} %param.23) | copy-start | bytes 3145732
  56.6 1.2 copy-start.11
  57.8 1.2 copy-start.12
  61.9 0.7 copy-start.6
  61.9 1.4 copy-start.7
  61.9 2.1 copy-start.8
  61.9 2.8 %copy-start.13 = (f32[4]{0:T(128)S(1)}, f32[4]{0:T(128)}, u32[]{:S(2)}) copy-start(f32[4]{0:T(128)} %param.27) | copy-start | bytes 52
  61.9 2.8 %copy-start.3 = (bf16[48,4,4,128]{3,2,1,0:T(4,128)(2,1)S(1)}, bf16[48,4,4,128]{3,2,1,0:T(4,128)(2,1)}, u32[]{:S(2)}) copy-start(bf16[48,4,4,128]{3,2,1,0:T(4,128)(2,1)} %param.34) | copy-start | bytes 589828
  61.9 2.8 %copy-start.4 = (bf16[48,4,4,128]{3,2,1,0:T(4,128)(2,1)S(1)}, bf16[48,4,4,128]{3,2,1,0:T(4,128)(2,1)}, u32[]{:S(2)}) copy-start(bf16[48,4,4,128]{3,2,1,0:T(4,128)(2,1)} %param.33) | copy-start | bytes 589828
  62.0 138.7 %reduce-scatter.8.cloned.1.call-start = ((), (), s32[]{:S(2)}) async-start(), calls=%async_computation.5 | async-start | bytes 1966080 | tf_op jit(solution)/shard_map/reduce_scatter | solution.py:253
  65.5 16.2 %copy-start.5 = (f32[48,4,4]{0,2,1:T(4,128)S(1)}, f32[48,4,4]{0,2,1:T(4,128)}, u32[]{:S(2)}) copy-start(f32[48,4,4]{0,2,1:T(4,128)} %param.29) | copy-start | bytes 9220
  65.5 16.2 %copy-start.9 = (f32[4]{0:T(128)S(1)}, f32[4]{0:T(128)}, u32[]{:S(2)}) copy-start(f32[4]{0:T(128)} %param.28) | copy-start | bytes 52
  200.7 22.5 %collective-permute-start.1 = (bf16[192,1024]{1,0:T(8,128)(2,1)}, bf16[192,1024]{1,0:T(8,128)(2,1)S(1)}, u32[]{:S(2)}, u32[]{:S(2)}) collective-permute-start(bf16[192,1024]{1,0:T(8,128)(2,1)} %reduce-scatter.8.cloned.1.call-done), channel_id=1, source_target_pairs={{0,0},{1,4},{2,8},{3,12},{4,1},{5,5},{6,9},{7,13},{8,2},{9,6},{10,... | collective-permute-start | bytes 1179656 | tf_op jit(solution)/shard_map/ppermute | solution.py:254
Sparse Core Ops, SparseCore 0:
  30.7 18.7 all-gather.1
  54.4 18.6 reduce-scatter.9
  75.3 61.1 reduce-scatter.5
  172.4 28.2 reduce-scatter.7

commit v2 on v1

--- a/solution.py
+++ b/solution.py
@@ -24,9 +24,10 @@
     return lax.broadcasted_iota(jnp.int32, (8, DK), 0) < P_SIZE
 
 
-def load_heads(heads, src, dst):
+def load_heads(heads, src, dst, factor=None):
     for h in range(heads):
-        dst[pl.ds(h * TALL, TALL), :] = src[:, h * DK : (h + 1) * DK].astype(f32)
+        part = src[:, h * DK : (h + 1) * DK].astype(f32)
+        dst[pl.ds(h * TALL, TALL), :] = part if factor is None else (part * factor).astype(bf16).astype(f32)
 
 
 def tile(h, pair):
@@ -87,9 +88,9 @@
                 o_ref[seq, h] = c_scr[pl.ds(h * SB + seq, 1), :] * s_ref[seq, h] + add
 
 
-def attend_kernel(heads, s_ref, q_ref, k_ref, v_ref, z_ref, d_ref, b_ref, w_ref, o_ref, rk, rq, qf, kf, vf, zf, of):
+def attend_kernel(heads, s_ref, a_ref, q_ref, k_ref, v_ref, z_ref, d_ref, b_ref, w_ref, o_ref, rk, rq, qf, kf, vf, zf, of):
     for src, dst in ((q_ref, qf), (k_ref, kf), (v_ref, vf), (z_ref, zf)):
-        load_heads(heads, src, dst)
+        load_heads(heads, src, dst, a_ref[...])
     low = first_half()
     for pair in range(SB // 2):
         for h in range(heads):
@@ -148,7 +149,7 @@
     )(state, keys, values, forgetting, strengths, counts)
 
 
-def attend(state, packed, decay, beta, gain):
+def attend(state, packed, factor, decay, beta, gain):
     seqs, heads = state.shape[:2]
     width = heads * DK
     rows = TALL
@@ -161,13 +162,195 @@
     return pl.pallas_call(
         functools.partial(attend_kernel, heads),
         grid=(seqs // SB,),
-        in_specs=[block, part(0), part(1), part(2), part(3), thin, thin, pl.BlockSpec((1, DK), lambda i: (0, 0))],
+        in_specs=[block, pl.BlockSpec((rows, 1), lambda i: (i, 0)), part(0), part(1), part(2), part(3), thin, thin, pl.BlockSpec((1, DK), lambda i: (0, 0))],
         out_specs=pl.BlockSpec((rows, width), lambda i: (i, 0)),
         out_shape=jax.ShapeDtypeStruct((seqs * P_SIZE, width), bf16),
         scratch_shapes=[pltpu.VMEM((heads * TALL, DK), f32)] * 7,
         cost_estimate=pl.CostEstimate(flops=5_000_000_000, bytes_accessed=state.size * 4, transcendentals=0),
         name="attend",
-    )(state, packed, packed, packed, packed, decay, beta, gain.reshape(1, DK))
+    )(state, factor, packed, packed, packed, packed, decay, beta, gain.reshape(1, DK))
+
+
+def pick(index, values):
+    chosen = values[-1]
+    for at, value in enumerate(values[:-1]):
+        chosen = jnp.where(index == at, value, chosen)
+    return chosen
+
+
+def turned_slot(t):
+    return pick(t, (0, 2, 1, 3))
+
+
+ORDER = ((3, 2, 1, 0), (0, 2, 1, 3), (3, 1, 2, 0), (0, 1, 2, 3))
+
+
+def project_kernel(x_ref, gain_ref, wq, wk, wv, wz, wf, ws, acc, few_ref, xbuf, w, fs, send, recv, esend, erecv,
+                   xs, xr, wsem, ps, pr, es, er):
+    k, t, g = lax.axis_index("kv"), lax.axis_index("tp"), lax.axis_index("grp")
+    depth, width = w.shape[1], w.shape[2]
+    rows = x_ref.shape[0]
+
+    def at(kv, tp):
+        return {"grp": g, "kv": kv, "tp": tp}
+
+    def remote(src, dst, ss, rs, kv, tp):
+        return pltpu.make_async_remote_copy(src, dst, ss, rs, device_id=at(kv, tp), device_id_type=pl.DeviceIdType.MESH)
+
+    loads = [pltpu.make_async_copy(src, w.at[i], wsem.at[i]) for i, src in enumerate((wq, wk, wv, wz))]
+    here = pl.ds(k * depth, depth)
+    loads += [pltpu.make_async_copy(src.at[here], fs.at[i], wsem.at[4 + i]) for i, src in enumerate((wf, ws))]
+    slot = turned_slot(t)
+    far_t, far_k = turned_slot(k), t
+    home = jnp.logical_and(far_k == k, far_t == t)
+    first = remote(x_ref, xbuf.at[k], xs.at[0], xr.at[k], far_k, far_t)
+    local = pltpu.make_async_copy(x_ref, xbuf.at[k], xr.at[k])
+
+    @pl.when(jnp.logical_not(home))
+    def _():
+        first.start()
+
+    @pl.when(home)
+    def _():
+        local.start()
+
+    for load in loads:
+        load.start()
+
+    beside = t + 1 - 2 * (t % 2)
+    across = (t + 2) % 4
+
+    def arrived(s):
+        remote(xbuf.at[s], xbuf.at[s], xs.at[0], xr.at[s], k, beside).wait_recv()
+
+    @pl.when(home)
+    def _():
+        local.wait()
+
+    @pl.when(jnp.logical_not(home))
+    def _():
+        arrived(slot)
+
+    over = remote(xbuf.at[slot], xbuf.at[slot], xs.at[1], xr.at[slot], k, across)
+    over.start()
+    near = remote(xbuf.at[slot], xbuf.at[slot], xs.at[2], xr.at[slot], k, beside)
+    near.start()
+    other = turned_slot(across)
+    arrived(other)
+    onward = remote(xbuf.at[other], xbuf.at[other], xs.at[3], xr.at[other], k, beside)
+    onward.start()
+    arrived(turned_slot(beside))
+    arrived(turned_slot((beside + 2) % 4))
+    for load in loads:
+        load.wait()
+
+    def step(i, carry):
+        r = pick(k, [pick(i, row) for row in ORDER])
+        own = r == k
+        floated = xbuf[r].astype(f32)
+        gained = (floated * gain_ref[k]).astype(bf16)
+        squares = floated * floated
+        high = squares.astype(bf16)
+        rest = (squares - high.astype(f32)).astype(bf16)
+        ones = jnp.ones((8, depth), bf16)
+        nt = (((1,), (1,)), ((), ()))
+        tn = (((0,), (1,)), ((), ()))
+        esend[r, 0:16, :] = lax.dot_general(fs[0], gained, tn, preferred_element_type=f32)
+        esend[r, 16:32, :] = lax.dot_general(fs[1], gained, tn, preferred_element_type=f32)
+        esend[r, 32:40, :] = lax.dot_general(ones, high, nt, preferred_element_type=f32) + lax.dot_general(
+            ones, rest, nt, preferred_element_type=f32
+        )
+        for j in range(4):
+            part = jnp.dot(gained, w[j], preferred_element_type=f32)
+            cols = slice(j * width, (j + 1) * width)
+
+            @pl.when(own)
+            def _():
+                acc[:, cols] = part
+
+            @pl.when(jnp.logical_not(own))
+            def _():
+                send[r, :, cols] = part.astype(bf16)
+
+        relayed = jnp.logical_or(jnp.logical_and(k == 1, r == 3), jnp.logical_and(k == 2, r == 0))
+
+        @pl.when(relayed)
+        def _():
+            remote(send.at[r], recv.at[4], ps.at[r], pr.at[4], k, beside).wait_recv()
+
+            def add(c, carry):
+                at_rows = pl.ds(c * 16, 16)
+                send[r, at_rows, :] = (send[r, at_rows, :].astype(f32) + recv[4, at_rows, :].astype(f32)).astype(bf16)
+                return carry
+
+            lax.fori_loop(0, rows // 16, add, 0)
+
+        @pl.when(jnp.logical_not(own))
+        def _():
+            ends = jnp.logical_or(jnp.logical_and(k == 0, r == 3), jnp.logical_and(k == 3, r == 0))
+            target = jnp.where(ends, jnp.where(k == 0, 1, 2), r)
+            place = jnp.where(ends, 4, k)
+            remote(send.at[r], recv.at[place], ps.at[r], pr.at[place], target, t).start()
+            remote(esend.at[r], erecv.at[k], es.at[r], er.at[k], r, t).start()
+
+        return carry
+
+    lax.fori_loop(0, 4, step, 0)
+
+    first_wait = jnp.logical_not(home)
+
+    @pl.when(first_wait)
+    def _():
+        first.wait_send()
+
+    over.wait_send()
+    near.wait_send()
+    onward.wait_send()
+
+    few_ref[...] = esend[k]
+    for src in range(4):
+
+        @pl.when(k != src)
+        def _():
+            remote(esend.at[src], erecv.at[src], es.at[src], er.at[src], k, beside).wait()
+            few_ref[...] += erecv[src]
+            remote(send.at[src], recv.at[src], ps.at[src], pr.at[src], k, beside).wait_send()
+
+        @pl.when(jnp.logical_and(k != src, k + src != 3) if src in (0, 3) else k != src)
+        def _():
+            remote(send.at[src], recv.at[src], ps.at[src], pr.at[src], k, beside).wait_recv()
+
+            def add(c, carry):
+                at_rows = pl.ds(c * 16, 16)
+                acc[at_rows, :] = acc[at_rows, :] + recv[src, at_rows, :].astype(f32)
+                return carry
+
+            lax.fori_loop(0, rows // 16, add, 0)
+
+
+def project(x, gain, weights, forgetting, strength):
+    rows, depth = x.shape
+    width = weights[0].shape[1]
+    vmem, hbm = pl.BlockSpec(memory_space=pltpu.VMEM), pl.BlockSpec(memory_space=pl.ANY)
+    dma = pltpu.SemaphoreType.DMA
+    return pl.pallas_call(
+        project_kernel,
+        in_specs=[vmem, vmem] + [hbm] * 6,
+        out_specs=[vmem, vmem],
+        out_shape=[jax.ShapeDtypeStruct((rows, 4 * width), f32), jax.ShapeDtypeStruct((40, rows), f32)],
+        scratch_shapes=[
+            pltpu.VMEM((4, rows, depth), bf16),
+            pltpu.VMEM((4, depth, width), bf16),
+            pltpu.VMEM((2,) + (depth, forgetting.shape[1]), bf16),
+            pltpu.VMEM((4, rows, 4 * width), bf16),
+            pltpu.VMEM((5, rows, 4 * width), bf16),
+            pltpu.VMEM((4, 40, rows), f32),
+            pltpu.VMEM((4, 40, rows), f32),
+            dma((4,)), dma((4,)), dma((6,)), dma((4,)), dma((5,)), dma((4,)), dma((4,)),
+        ],
+        compiler_params=pltpu.CompilerParams(has_side_effects=True, vmem_limit_bytes=56 * 2**20),
+        name="project",
+    )(x, gain.reshape(-1, 1, depth), *weights, forgetting, strength)
 
 
 def on_device(
@@ -205,33 +388,34 @@
     def thin(values):
         return values.reshape(seqs, P_SIZE * heads)
 
-    if square:
-        turned = lax.ppermute(candidate_embeddings, ("kv", "tp"), swap)
-        every = lax.all_gather(turned, "tp", axis=0, tiled=True)
+    weights = (probe_projector, address_projector, content_projector, sigmoid_mask_matrix)
+    if n_kv == 4 and n_tp == 4:
+        summed, few = project(
+            candidate_embeddings, incoming_rms_scaling, weights, forgetting_projector, strength_projector_matrix
+        )
+        columns = forgetting_projector.shape[1]
+        few = [lax.dynamic_slice_in_dim(few, n * columns + t_index * heads, heads) for n in range(2)] + [few[2 * columns : 2 * columns + 1]]
+        few = jnp.concatenate(few, axis=0).T
     else:
         every = lax.all_gather(candidate_embeddings, "tp", axis=1, tiled=True)
         every = lax.all_to_all(every, "kv", split_axis=1, concat_axis=0, tiled=True)
-    gain_part = lax.dynamic_slice_in_dim(incoming_rms_scaling, k_index * depth, depth)
-    floated = every.astype(f32)
-    gained = (floated * gain_part).astype(bf16)
-    decay_cols = lax.dynamic_slice(forgetting_projector, (k_index * depth, t_index * heads), (depth, heads))
-    beta_cols = lax.dynamic_slice(strength_projector_matrix, (k_index * depth, t_index * heads), (depth, heads))
-    few = jnp.concatenate(
-        [
-            jnp.dot(gained, jnp.concatenate([decay_cols, beta_cols], axis=1), preferred_element_type=f32),
-            jnp.sum(floated * floated, axis=1, keepdims=True),
-        ],
-        axis=1,
-    )
-    few = lax.psum_scatter(few, "kv", scatter_dimension=0, tiled=True)
-    partial = jnp.concatenate(
-        [
-            jnp.dot(gained, w, preferred_element_type=f32).astype(bf16)
-            for w in (probe_projector, address_projector, content_projector, sigmoid_mask_matrix)
-        ],
-        axis=1,
-    )
-    summed = lax.psum_scatter(partial, "kv", scatter_dimension=0, tiled=True)
+        gain_part = lax.dynamic_slice_in_dim(incoming_rms_scaling, k_index * depth, depth)
+        floated = every.astype(f32)
+        gained = (floated * gain_part).astype(bf16)
+        decay_cols = lax.dynamic_slice(forgetting_projector, (k_index * depth, t_index * heads), (depth, heads))
+        beta_cols = lax.dynamic_slice(strength_projector_matrix, (k_index * depth, t_index * heads), (depth, heads))
+        few = jnp.concatenate(
+            [
+                jnp.dot(gained, jnp.concatenate([decay_cols, beta_cols], axis=1), preferred_element_type=f32),
+                jnp.sum(floated * floated, axis=1, keepdims=True),
+            ],
+            axis=1,
+        )
+        few = lax.psum_scatter(few, "kv", scatter_dimension=0, tiled=True)
+        partial = jnp.concatenate(
+            [jnp.dot(gained, w, preferred_element_type=f32).astype(bf16) for w in weights], axis=1
+        )
+        summed = lax.psum_scatter(partial, "kv", scatter_dimension=0, tiled=True).astype(f32)
     taken = accepted(
         memory_matrix,
         earlier_addresses.reshape(rows, width),
@@ -242,11 +426,10 @@
     )
     factor = lax.rsqrt(few[:, 2 * heads :] / features + epsilon)
     few = few[:, : 2 * heads] * factor
-    packed = (summed.astype(f32) * factor).astype(bf16)
     decay_in = few[:, :heads].reshape(seqs, P_SIZE, heads)
     beta = jax.nn.sigmoid(few[:, heads:].reshape(seqs, P_SIZE, heads))
     decay = -jnp.exp(channel_forgetting_rates) * jax.nn.softplus(decay_in + forgetting_offset) + extra_forgetting
-    flat = attend(taken, packed, thin(decay), thin(beta), outgoing_rms_scaling)
+    flat = attend(taken, summed, factor, thin(decay), thin(beta), outgoing_rms_scaling)
     gathered = lax.all_gather(flat, "kv", axis=0, tiled=True)
     terms = jnp.dot(gathered, final_projector, preferred_element_type=f32).astype(bf16)
     if square:

time: 232 us -> 220 us (0.948)
  Pallas kernels: 27 us -> 117 us
  waiting for transfers between devices: 138 us -> 48.1 us
  matrix products: 9.32 us -> 2.15 us
  other arithmetic: 7.13 us -> 1.78 us
  starting transfers between devices: 6.76 us -> 3.6 us
    pallas_call x0 -> x1, Pallas kernels: none -> 91.3 us  [project(): pl.pallas_call(project_kernel, in_specs=[vmem, vmem] + [hbm] * 6, out_spe...]
    reduce_scatter x1 -> x0, waiting for transfers between devices: 54.1 us -> none  [on_device(): summed = lax.psum_scatter(partial, 'kv', scatter_dimension=0, tiled=True)]
    ppermute x1 -> x0, waiting for transfers between devices: 19.5 us -> none  [on_device(): turned = lax.ppermute(candidate_embeddings, ('kv', 'tp'), swap)]
    all_gather x1 -> x0, waiting for transfers between devices: 16.5 us -> none  [on_device(): every = lax.all_gather(turned, 'tp', axis=0, tiled=True)]
    dot_general x5 -> x0, matrix products: 7.15 us -> none  [the longest x4 5.23 us: on_device(): jnp.dot(gained, w, preferred_element_type=f32).astype(bf16)]
    ppermute x1 -> x0, starting transfers between devices: 3.03 us -> none  [on_device(): turned = lax.ppermute(candidate_embeddings, ('kv', 'tp'), swap)]
    unnamed x32 -> x13, local copies, waits for them, and re-layouts: 4.56 us -> 5.21 us
  transfers between devices with their start and end apart: 6 -> 2, of which waited for: 5 -> 2; matrix products, arithmetic and copies ran while one was open for 7% -> 0% of each run, Pallas kernels for 6% -> 0%
where the time goes in v2:
time: 220 us; the launch traced here: 219 us
  Pallas kernels  117 us (53%)
  waiting for transfers between devices  48.1 us (22%)
  blocking collectives  18.7 us (8%)
  between operations  14.1 us (6%)
  local copies, waits for them, and re-layouts  13.1 us (6%)
  starting transfers between devices  3.6 us (2%)
    pallas_call x1, Pallas kernels, project(): pl.pallas_call(project_kernel, in_specs=[vmem, vmem] + [hbm] * 6, out_spe...  91.3 us
    reduce_scatter x1, waiting for transfers between devices, on_device(): mixed = lax.psum_scatter(terms, 'tp', scatter_dimension=0, tiled=True)  29.1 us
    ppermute x1, waiting for transfers between devices, on_device(): mixed = lax.ppermute(mixed, ('kv', 'tp'), swap)  19 us
    all_gather x1, blocking collectives, on_device(): gathered = lax.all_gather(flat, 'kv', axis=0, tiled=True)  18.7 us
    pallas_call x1, Pallas kernels, accepted(): pl.pallas_call(functools.partial(accepted_kernel, heads), grid=(seqs // S...  13 us
    pallas_call x1, Pallas kernels, attend(): pl.pallas_call(functools.partial(attend_kernel, heads), grid=(seqs // SB,...  12.9 us
    unnamed x13, local copies, waits for them, and re-layouts  5.21 us
  transfers between devices with their start and end apart: 2, of which 2 were waited for; matrix products, arithmetic and copies ran while one was open for 0% of the time, Pallas kernels for 0%

profile of v2, /device:TPU:10, one launch (start us, length us, event | category | flops | bytes accessed | tf_op | source)
XLA Modules:
  0.0 218.7 jit_solution(13100739900466030284)
XLA Ops:
  7.2 0.0 copy-start
  7.2 0.0 reduce-scatter.2.cloned.1.call-start
  7.2 0.7 exponential_negate_fusion
  8.0 1.4 copy.50.b_ref
  9.3 1.4 copy.49.f_ref
  10.7 1.3 copy.51.n_ref
  12.1 2.2 %copy.52.wf = bf16[4096,16]{1,0:T(8,128)(2,1)} copy(bf16[4096,16]{0,1:T(8,128)(2,1)} %param.25) | data formatting | bytes 262144 | tf_op args[6]
  14.3 2.2 %copy.53.ws = bf16[4096,16]{1,0:T(8,128)(2,1)} copy(bf16[4096,16]{0,1:T(8,128)(2,1)} %param.26) | data formatting | bytes 262144 | tf_op args[7]
  16.5 0.0 copy-start.3
  16.5 0.0 copy-start.4
  16.5 0.0 copy-start.1
  16.5 0.0 copy-start.2
  16.5 91.3 %project.1 = (f32[192,2048]{1,0:T(8,128)}, f32[40,192]{1,0:T(8,128)}) custom-call(bf16[192,1024]{1,0:T(8,128)(2,1)} %x_ref.1, f32[4,1,1024]{2,1,0:T(1,128)} %bitcast.24, bf16[1024,512]{1,0:T(8,128)(2,1)} %wq.1, bf16[1024,512]{1,0:T(8,128)(2,1)} %wk.1, bf16[1024,512]{1,0:T(8,128)(2,1)} %wv.1, bf16[1024,512]{1,0:T(8,128)(2,1)} %wz.1, ...), custom_call_target="tpu_custom_call" | custom-call | tf_op jit(solution)/shard_map/project/pallas_call | solution.py:336
  107.8 0.7 slice.15
  108.5 0.7 constant_dynamic-slice_fusion.1
  109.2 0.1 copy.54
  109.3 0.7 fusion.7
  110.1 0.1 slice_multiply_fusion
  110.2 0.1 fusion.2
  110.3 0.7 div.16.b_ref
  111.0 0.1 copy.55
  111.1 0.0 copy-done.3
  111.1 0.0 copy-done.4
  111.1 0.1 fusion.6
  111.2 0.7 copy.58.d_ref
  111.9 0.0 copy-done.1
  111.9 0.0 copy-done.2
  111.9 0.8 copy_bitcast_fusion
  112.7 13.0 %accepted.1.s_ref = f32[48,4,128,128]{3,2,1,0:T(8,128)} custom-call(f32[48,4,128,128]{3,2,1,0:T(8,128)} %s_ref.1, bf16[192,512]{1,0:T(8,128)(2,1)} %get-tuple-element.13.k_ref, bf16[192,512]{1,0:T(8,128)(2,1)} %get-tuple-element.12.v_ref, f32[48,16]{1,0:T(8,128)} %copy.49.f_ref, f32[48,16]{1,0:T(8,128)} %copy.50.b_ref, s32[48,1]{1,0:T(8,128)} %copy.51.n_ref), custom_call_target="tpu_custom_call" | custom-call | flops 10000000000 | bytes 25165824 | tf_op jit(solution)/shard_map/accepted/pallas_call | solution.py:140
  125.7 12.9 %attend.1 = bf16[192,512]{1,0:T(8,128)(2,1)} custom-call(f32[48,4,128,128]{3,2,1,0:T(8,128)} %accepted.1.s_ref, f32[192,1]{1,0:T(8,128)} %get-tuple-element.9.a_ref, f32[192,2048]{1,0:T(8,128)} %get-tuple-element.5.q_ref.k_ref.v_ref.z_ref, f32[192,2048]{1,0:T(8,128)} %get-tuple-element.5.q_ref.k_ref.v_ref.z_ref, ...), custom_call_target="tpu_custom_call" | custom-call | flops 5000000000 | bytes 12582912 | tf_op jit(solution)/shard_map/attend/pallas_call | solution.py:162
  138.6 18.7 %all_gather.3 = bf16[768,512]{1,0:T(8,128)(2,1)S(1)} all-gather(bf16[192,512]{1,0:T(8,128)(2,1)} %attend.1), channel_id=1, replica_groups=mesh['grp'=2,'kv'=4,'tp'=4] {'kv'}, dimensions={0}, use_global_device_ids=true | all-gather | bytes 983040 | tf_op jit(solution)/shard_map/all_gather | solution.py:433
  157.3 0.0 copy-done
  157.3 2.2 convolution_convert_fusion
  159.4 0.0 reduce-scatter.2.cloned.1.call-update
  159.5 29.1 %reduce-scatter.2.cloned.1.call-done = bf16[192,1024]{1,0:T(8,128)(2,1)} async-done(((bf16[768,1024]{1,0:T(8,128)(2,1)}), bf16[192,1024]{1,0:T(8,128)(2,1)}) %reduce-scatter.2.cloned.1.call-update) | async-done | bytes 393232 | tf_op jit(solution)/shard_map/reduce_scatter | solution.py:436
  188.5 3.6 %collective-permute-start = (bf16[192,1024]{1,0:T(8,128)(2,1)}, bf16[192,1024]{1,0:T(8,128)(2,1)S(1)}, u32[]{:S(2)}, u32[]{:S(2)}) collective-permute-start(bf16[192,1024]{1,0:T(8,128)(2,1)} %reduce-scatter.2.cloned.1.call-done), channel_id=1, source_target_pairs={{0,0},{1,4},{2,8},{3,12},{4,1},{5,5},{6,9},{7,13},{8,2},{9,6},{10,... | collective-permute-start | bytes 1179656 | tf_op jit(solution)/shard_map/ppermute | solution.py:437
  192.1 19.0 %collective-permute-done = bf16[192,1024]{1,0:T(8,128)(2,1)S(1)} collective-permute-done((bf16[192,1024]{1,0:T(8,128)(2,1)}, bf16[192,1024]{1,0:T(8,128)(2,1)S(1)}, u32[]{:S(2)}, u32[]{:S(2)}) %collective-permute-start) | collective-permute-done | bytes 393248 | tf_op jit(solution)/shard_map/ppermute | solution.py:437
  211.1 0.7 copy.64
  (1 shorter events, 0.0 us)
Async XLA Ops:
  7.2 150.1 %copy-start = (bf16[512,1024]{1,0:T(8,128)(2,1)S(1)}, bf16[512,1024]{1,0:T(8,128)(2,1)}, u32[]{:S(2)}) copy-start(bf16[512,1024]{1,0:T(8,128)(2,1)} %param.31) | copy-start | bytes 3145732
  7.2 181.3 %reduce-scatter.2.cloned.1.call-start = ((), (), s32[]{:S(2)}) async-start(), calls=%async_computation.1 | async-start | bytes 1966080 | tf_op jit(solution)/shard_map/reduce_scatter | solution.py:436
  16.5 94.6 %copy-start.3 = (f32[48,4,4]{0,2,1:T(4,128)S(1)}, f32[48,4,4]{0,2,1:T(4,128)}, u32[]{:S(2)}) copy-start(f32[48,4,4]{0,2,1:T(4,128)} %param.29) | copy-start | bytes 9220
  16.5 94.6 %copy-start.4 = (f32[4]{0:T(128)S(1)}, f32[4]{0:T(128)}, u32[]{:S(2)}) copy-start(f32[4]{0:T(128)} %param.28) | copy-start | bytes 52
  16.5 95.4 %copy-start.1 = (bf16[48,4,4,128]{3,2,1,0:T(4,128)(2,1)S(1)}, bf16[48,4,4,128]{3,2,1,0:T(4,128)(2,1)}, u32[]{:S(2)}) copy-start(bf16[48,4,4,128]{3,2,1,0:T(4,128)(2,1)} %param.34) | copy-start | bytes 589828
  16.5 95.4 %copy-start.2 = (bf16[48,4,4,128]{3,2,1,0:T(4,128)(2,1)S(1)}, bf16[48,4,4,128]{3,2,1,0:T(4,128)(2,1)}, u32[]{:S(2)}) copy-start(bf16[48,4,4,128]{3,2,1,0:T(4,128)(2,1)} %param.33) | copy-start | bytes 589828
  188.5 22.5 %collective-permute-start = (bf16[192,1024]{1,0:T(8,128)(2,1)}, bf16[192,1024]{1,0:T(8,128)(2,1)S(1)}, u32[]{:S(2)}, u32[]{:S(2)}) collective-permute-start(bf16[192,1024]{1,0:T(8,128)(2,1)} %reduce-scatter.2.cloned.1.call-done), channel_id=1, source_target_pairs={{0,0},{1,4},{2,8},{3,12},{4,1},{5,5},{6,9},{7,13},{8,2},{9,6},{10,... | collective-permute-start | bytes 1179656 | tf_op jit(solution)/shard_map/ppermute | solution.py:437
Sparse Core Ops, SparseCore 0:
  159.6 28.9 reduce-scatter.1

commit v3 on v2

--- a/solution.py
+++ b/solution.py
@@ -38,7 +38,7 @@
     return pl.ds(h * TALL + p, SB, stride=P_SIZE)
 
 
-def accepted_kernel(heads, s_ref, k_ref, v_ref, f_ref, b_ref, n_ref, o_ref, r_scr, u_scr, c_scr, kf, vf):
+def accepted_kernel(heads, s_ref, k_ref, v_ref, n_ref, o_ref, r_scr, u_scr, c_scr, kf, vf):
     load_heads(heads, k_ref, kf)
     load_heads(heads, v_ref, vf)
     low = first_half()
@@ -49,7 +49,9 @@
             r0 = jnp.dot(lhs, s_ref[2 * pair, h].astype(bf16), preferred_element_type=f32)
             r1 = jnp.dot(lhs, s_ref[2 * pair + 1, h].astype(bf16), preferred_element_type=f32)
             r_scr[at, :] = jnp.where(low, r0, r1)
-    count = n_ref[...]
+    few = n_ref[...]
+    span = P_SIZE * heads
+    count = few[:, 2 * span : 2 * span + 1]
     for h in range(heads):
         scale = jnp.ones((SB, 1), f32)
         ks, us, norms = [], [], []
@@ -58,9 +60,9 @@
             col = slice(p * heads + h, p * heads + h + 1)
             key = kf[at, :]
             norm = lax.rsqrt(lane_dot(key, key) + epsilon)
-            live = count > p
-            g = jnp.where(live, jnp.exp(f_ref[:, col]), 1.0)
-            b = jnp.where(live, b_ref[:, col], 0.0)
+            live = count > float(p)
+            g = jnp.where(live, jnp.exp(few[:, p * heads + h : p * heads + h + 1]), 1.0)
+            b = jnp.where(live, few[:, span + p * heads + h : span + p * heads + h + 1], 0.0)
             rec = (scale * norm) * r_scr[at, :]
             for ki, ui, ni in zip(ks, us, norms):
                 rec = rec + (lane_dot(ki, key) * (ni * norm)) * ui
@@ -130,23 +132,23 @@
         o_ref[:, h * DK : (h + 1) * DK] = of[pl.ds(h * TALL, TALL), :].astype(bf16)
 
 
-def accepted(state, keys, values, forgetting, strengths, counts):
+def accepted(state, keys, values, few):
     seqs, heads = state.shape[:2]
     width = heads * DK
     rows = TALL
     tall = pl.BlockSpec((rows, width), lambda i: (i, 0))
-    thin = pl.BlockSpec((SB, P_SIZE * heads), lambda i: (i, 0))
+    thin = pl.BlockSpec((SB, few.shape[1]), lambda i: (i, 0))
     block = pl.BlockSpec((SB, heads, DK, DK), lambda i: (i, 0, 0, 0))
     return pl.pallas_call(
         functools.partial(accepted_kernel, heads),
         grid=(seqs // SB,),
-        in_specs=[block, tall, tall, thin, thin, pl.BlockSpec((SB, 1), lambda i: (i, 0))],
+        in_specs=[block, tall, tall, thin],
         out_specs=block,
         out_shape=jax.ShapeDtypeStruct(state.shape, f32),
         scratch_shapes=[pltpu.VMEM((heads * n, DK), f32) for n in (TALL, TALL, SB, TALL, TALL)],
         cost_estimate=pl.CostEstimate(flops=10_000_000_000, bytes_accessed=2 * state.size * 4, transcendentals=0),
         name="accepted",
-    )(state, keys, values, forgetting, strengths, counts)
+    )(state, keys, values, few)
 
 
 def attend(state, packed, factor, decay, beta, gain):
@@ -199,7 +201,7 @@
 
     loads = [pltpu.make_async_copy(src, w.at[i], wsem.at[i]) for i, src in enumerate((wq, wk, wv, wz))]
     here = pl.ds(k * depth, depth)
-    loads += [pltpu.make_async_copy(src.at[here], fs.at[i], wsem.at[4 + i]) for i, src in enumerate((wf, ws))]
+    loads += [pltpu.make_async_copy(src.at[:, here], fs.at[i], wsem.at[4 + i]) for i, src in enumerate((wf, ws))]
     slot = turned_slot(t)
     far_t, far_k = turned_slot(k), t
     home = jnp.logical_and(far_k == k, far_t == t)
@@ -254,9 +256,8 @@
         rest = (squares - high.astype(f32)).astype(bf16)
         ones = jnp.ones((8, depth), bf16)
         nt = (((1,), (1,)), ((), ()))
-        tn = (((0,), (1,)), ((), ()))
-        esend[r, 0:16, :] = lax.dot_general(fs[0], gained, tn, preferred_element_type=f32)
-        esend[r, 16:32, :] = lax.dot_general(fs[1], gained, tn, preferred_element_type=f32)
+        esend[r, 0:16, :] = lax.dot_general(fs[0], gained, nt, preferred_element_type=f32)
+        esend[r, 16:32, :] = lax.dot_general(fs[1], gained, nt, preferred_element_type=f32)
         esend[r, 32:40, :] = lax.dot_general(ones, high, nt, preferred_element_type=f32) + lax.dot_general(
             ones, rest, nt, preferred_element_type=f32
         )
@@ -341,7 +342,7 @@
         scratch_shapes=[
             pltpu.VMEM((4, rows, depth), bf16),
             pltpu.VMEM((4, depth, width), bf16),
-            pltpu.VMEM((2,) + (depth, forgetting.shape[1]), bf16),
+            pltpu.VMEM((2, forgetting.shape[1], depth), bf16),
             pltpu.VMEM((4, rows, 4 * width), bf16),
             pltpu.VMEM((5, rows, 4 * width), bf16),
             pltpu.VMEM((4, 40, rows), f32),
@@ -350,7 +351,128 @@
         ],
         compiler_params=pltpu.CompilerParams(has_side_effects=True, vmem_limit_bytes=56 * 2**20),
         name="project",
-    )(x, gain.reshape(-1, 1, depth), *weights, forgetting, strength)
+    )(x, gain.reshape(-1, 1, depth), *weights, forgetting.T, strength.T)
+
+
+NEAREST = ((0, 1, 2, 3), (1, 0, 2, 3), (2, 3, 1, 0), (3, 2, 1, 0))
+
+
+def mix_kernel(flat_ref, wo, o_ref, held, w, part, mate, cross, total, wsem, gs, gr, ms, mr, xs, xr, ts, tr):
+    k, t, g = lax.axis_index("kv"), lax.axis_index("tp"), lax.axis_index("grp")
+    rows = flat_ref.shape[0]
+
+    def remote(src, dst, ss, rs, kv, tp):
+        return pltpu.make_async_remote_copy(
+            src, dst, ss, rs, device_id={"grp": g, "kv": kv, "tp": tp}, device_id_type=pl.DeviceIdType.MESH
+        )
+
+    load = pltpu.make_async_copy(wo, w, wsem.at[0])
+    own = pltpu.make_async_copy(flat_ref, held.at[k], wsem.at[1])
+    own.start()
+    sends = [remote(flat_ref, held.at[k], gs.at[n], gr.at[k], lax.rem(k + n, 4), t) for n in (1, 2, 3)]
+    for copy in sends:
+        copy.start()
+    load.start()
+    beside = t + 1 - 2 * (t % 2)
+    across = (t + 2) % 4
+    diagonal = (beside + 2) % 4
+    load.wait()
+    own.wait()
+
+    def to_mate(r, n):
+        return remote(part.at[r], mate.at[n], ms.at[n], mr.at[n], k, beside)
+
+    def to_cross(r):
+        return remote(part.at[r], cross, xs, xr, k, across)
+
+    def step(i, carry):
+        r = pick(k, [pick(i, row) for row in NEAREST])
+
+        @pl.when(r != k)
+        def _():
+            remote(held.at[r], held.at[r], gs.at[0], gr.at[r], r, t).wait_recv()
+
+        part[r] = jnp.dot(held[r], w[...], preferred_element_type=f32).astype(bf16)
+        sink = turned_slot(r)
+
+        @pl.when(sink == beside)
+        def _():
+            to_mate(r, 0).start()
+
+        @pl.when(sink == diagonal)
+        def _():
+            to_mate(r, 1).start()
+
+        @pl.when(sink == across)
+        def _():
+            to_mate(r, 1).wait_recv()
+
+            def add(c, carry):
+                at_rows = pl.ds(c * 16, 16)
+                part[r, at_rows, :] = (part[r, at_rows, :].astype(f32) + mate[1, at_rows, :].astype(f32)).astype(bf16)
+                return carry
+
+            lax.fori_loop(0, rows // 16, add, 0)
+            to_cross(r).start()
+
+        return carry
+
+    lax.fori_loop(0, 4, step, 0)
+    mine = turned_slot(t)
+    to_mate(mine, 0).wait_recv()
+    to_cross(mine).wait_recv()
+
+    def add(c, carry):
+        at_rows = pl.ds(c * 16, 16)
+        total[at_rows, :] = (
+            part[mine, at_rows, :].astype(f32) + mate[0, at_rows, :].astype(f32) + cross[at_rows, :].astype(f32)
+        ).astype(bf16)
+        return carry
+
+    lax.fori_loop(0, rows // 16, add, 0)
+    home = jnp.logical_and(mine == k, t == k)
+    last = remote(total, o_ref, ts, tr, mine, k)
+    local = pltpu.make_async_copy(total, o_ref, tr)
+
+    @pl.when(home)
+    def _():
+        local.start()
+        local.wait()
+
+    @pl.when(jnp.logical_not(home))
+    def _():
+        last.start()
+        last.wait()
+
+    for copy in sends:
+        copy.wait_send()
+    to_mate(0, 0).wait_send()
+    to_mate(0, 1).wait_send()
+    to_cross(0).wait_send()
+
+
+def mix(flat, final):
+    rows, width = flat.shape
+    cols = final.shape[1]
+    vmem, hbm = pl.BlockSpec(memory_space=pltpu.VMEM), pl.BlockSpec(memory_space=pl.ANY)
+    dma = pltpu.SemaphoreType.DMA
+    return pl.pallas_call(
+        mix_kernel,
+        in_specs=[vmem, hbm],
+        out_specs=vmem,
+        out_shape=jax.ShapeDtypeStruct((rows, cols), bf16),
+        scratch_shapes=[
+            pltpu.VMEM((4, rows, width), bf16),
+            pltpu.VMEM((width, cols), bf16),
+            pltpu.VMEM((4, rows, cols), bf16),
+            pltpu.VMEM((2, rows, cols), bf16),
+            pltpu.VMEM((rows, cols), bf16),
+            pltpu.VMEM((rows, cols), bf16),
+            dma((2,)), dma((4,)), dma((4,)), dma((2,)), dma((2,)), dma, dma, dma, dma,
+        ],
+        compiler_params=pltpu.CompilerParams(has_side_effects=True, vmem_limit_bytes=56 * 2**20),
+        name="mix",
+    )(flat, final)
 
 
 def on_device(
@@ -381,8 +503,6 @@
     depth, width = probe_projector.shape
     heads = width // DK
     seqs = rows // P_SIZE
-    square = n_kv == n_tp
-    swap = [(a * n_tp + b, b * n_tp + a) for a in range(n_kv) for b in range(n_tp)] if square else None
     k_index, t_index = lax.axis_index("kv"), lax.axis_index("tp")
 
     def thin(values):
@@ -420,9 +540,9 @@
         memory_matrix,
         earlier_addresses.reshape(rows, width),
         earlier_contents.reshape(rows, width),
-        thin(earlier_forgetting),
-        thin(earlier_strengths),
-        admitted_counts.reshape(seqs, 1),
+        jnp.concatenate(
+            [thin(earlier_forgetting), thin(earlier_strengths), admitted_counts.astype(f32).reshape(seqs, 1)], axis=1
+        ),
     )
     factor = lax.rsqrt(few[:, 2 * heads :] / features + epsilon)
     few = few[:, : 2 * heads] * factor
@@ -430,12 +550,11 @@
     beta = jax.nn.sigmoid(few[:, heads:].reshape(seqs, P_SIZE, heads))
     decay = -jnp.exp(channel_forgetting_rates) * jax.nn.softplus(decay_in + forgetting_offset) + extra_forgetting
     flat = attend(taken, summed, factor, thin(decay), thin(beta), outgoing_rms_scaling)
-    gathered = lax.all_gather(flat, "kv", axis=0, tiled=True)
-    terms = jnp.dot(gathered, final_projector, preferred_element_type=f32).astype(bf16)
-    if square:
-        mixed = lax.psum_scatter(terms, "tp", scatter_dimension=0, tiled=True)
-        mixed = lax.ppermute(mixed, ("kv", "tp"), swap)
+    if n_kv == 4 and n_tp == 4:
+        mixed = mix(flat, final_projector)
     else:
+        gathered = lax.all_gather(flat, "kv", axis=0, tiled=True)
+        terms = jnp.dot(gathered, final_projector, preferred_element_type=f32).astype(bf16)
         terms = lax.all_to_all(terms, "kv", split_axis=0, concat_axis=1, tiled=True)
         mixed = lax.psum_scatter(terms, "tp", scatter_dimension=1, tiled=True)
     return (mixed, taken)

time: 220 us -> 179 us (0.81)
  Pallas kernels: 117 us -> 167 us
  waiting for transfers between devices: 48.1 us -> 0 us
  blocking collectives: 18.7 us -> 0 us
  between operations: 14.1 us -> 0.7 us
  local copies, waits for them, and re-layouts: 13.1 us -> 8.22 us
  starting transfers between devices: 3.6 us -> 0 us
    pallas_call x0 -> x1, Pallas kernels: none -> 50.3 us  [mix(): pl.pallas_call(mix_kernel, in_specs=[vmem, hbm], out_specs=vmem, out_shap...]
    reduce_scatter x1 -> x0, waiting for transfers between devices: 29.1 us -> none  [on_device(): mixed = lax.psum_scatter(terms, 'tp', scatter_dimension=0, tiled=True)]
    ppermute x1 -> x0, waiting for transfers between devices: 19 us -> none  [on_device(): mixed = lax.ppermute(mixed, ('kv', 'tp'), swap)]
    all_gather x1 -> x0, blocking collectives: 18.7 us -> none  [on_device(): gathered = lax.all_gather(flat, 'kv', axis=0, tiled=True)]
    ppermute x1 -> x0, starting transfers between devices: 3.56 us -> none  [on_device(): mixed = lax.ppermute(mixed, ('kv', 'tp'), swap)]
    unnamed x13 -> x7, local copies, waits for them, and re-layouts: 5.21 us -> 1.78 us
  transfers between devices with their start and end apart: 2 -> 0, of which waited for: 2 -> 0; matrix products, arithmetic and copies ran while one was open for 0% -> 0% of each run, Pallas kernels for 0% -> 0%
where the time goes in v3:
time: 179 us; the launch traced here: 178 us
  Pallas kernels  167 us (93%)
  local copies, waits for them, and re-layouts  8.22 us (5%)
  other arithmetic  2.38 us (1%)
    pallas_call x1, Pallas kernels, project(): pl.pallas_call(project_kernel, in_specs=[vmem, vmem] + [hbm] * 6, out_spe...  91.2 us
    pallas_call x1, Pallas kernels, mix(): pl.pallas_call(mix_kernel, in_specs=[vmem, hbm], out_specs=vmem, out_shap...  50.3 us
    pallas_call x1, Pallas kernels, attend(): pl.pallas_call(functools.partial(attend_kernel, heads), grid=(seqs // SB,...  12.9 us
    pallas_call x1, Pallas kernels, accepted(): pl.pallas_call(functools.partial(accepted_kernel, heads), grid=(seqs // S...  12.7 us

profile of v3, /device:TPU:10, one launch (start us, length us, event | category | flops | bytes accessed | tf_op | source)
XLA Modules:
  0.0 178.5 jit_solution(7216380955844557774)
XLA Ops:
  0.6 1.8 %copy_bitcast_fusion = (bf16[192,512]{1,0:T(8,128)(2,1)}, bf16[192,512]{1,0:T(8,128)(2,1)}) fusion(bf16[24,8,4,128]{3,2,1,0:T(4,128)(2,1)} %bitcast.22, bf16[24,8,4,128]{3,2,1,0:T(4,128)(2,1)} %bitcast.23), kind=kLoop, calls=%fused_computation | loop fusion | bytes 786432 | tf_op jit(solution)/shard_map/reshape | solution.py:542
  2.4 0.7 convert_bitcast_fusion
  3.1 0.1 copy.45
  3.2 0.8 copy.44
  4.0 0.8 copy.43
  4.7 0.7 pad_maximum_fusion.n_ref
  5.4 0.0 copy-start.2
  5.4 0.0 copy-start
  5.4 0.0 copy-start.1
  5.4 12.7 %accepted.1.s_ref = f32[48,4,128,128]{3,2,1,0:T(8,128)} custom-call(f32[48,4,128,128]{3,2,1,0:T(8,128)} %s_ref.1, bf16[192,512]{1,0:T(8,128)(2,1)} %get-tuple-element.13.k_ref, bf16[192,512]{1,0:T(8,128)(2,1)} %get-tuple-element.12.v_ref, f32[48,33]{1,0:T(8,128)} %pad_maximum_fusion.n_ref), custom_call_target="tpu_custom_call" | custom-call | flops 10000000000 | bytes 25165824 | tf_op jit(solution)/shard_map/accepted/pallas_call | solution.py:142
  18.1 91.2 %project.1 = (f32[192,2048]{1,0:T(8,128)}, f32[40,192]{1,0:T(8,128)}) custom-call(bf16[192,1024]{1,0:T(8,128)(2,1)} %x_ref.1, f32[4,1,1024]{2,1,0:T(1,128)} %bitcast.27, bf16[1024,512]{1,0:T(8,128)(2,1)} %wq.1, bf16[1024,512]{1,0:T(8,128)(2,1)} %wk.1, bf16[1024,512]{1,0:T(8,128)(2,1)} %wv.1, bf16[1024,512]{1,0:T(8,128)(2,1)} %wz.1, ...), custom_call_target="tpu_custom_call" | custom-call | tf_op jit(solution)/shard_map/project/pallas_call | solution.py:337
  109.3 0.7 slice.15
  110.0 0.7 constant_dynamic-slice_fusion.1
  110.8 0.1 copy.46
  110.9 0.7 fusion.7
  111.6 0.1 slice_multiply_fusion
  111.7 0.1 fusion.2
  111.8 0.1 copy.47
  111.9 0.0 copy-done.2
  111.9 0.0 copy-done
  111.9 0.0 copy-done.1
  112.0 0.1 fusion.6
  112.0 0.7 copy.50.d_ref
  112.7 0.7 div.16.b_ref
  113.4 12.9 %attend.1.flat_ref = bf16[192,512]{1,0:T(8,128)(2,1)} custom-call(f32[48,4,128,128]{3,2,1,0:T(8,128)} %accepted.1.s_ref, f32[192,1]{1,0:T(8,128)} %get-tuple-element.9.a_ref, f32[192,2048]{1,0:T(8,128)} %get-tuple-element.5.q_ref.k_ref.v_ref.z_ref, f32[192,2048]{1,0:T(8,128)} %get-tuple-element.5.q_ref.k_ref.v_ref.z_ref, ...), custom_call_target="tpu_custom_call" | custom-call | flops 5000000000 | bytes 12582912 | tf_op jit(solution)/shard_map/attend/pallas_call | solution.py:164
  126.3 50.3 %mix.1 = bf16[192,1024]{1,0:T(8,128)(2,1)} custom-call(bf16[192,512]{1,0:T(8,128)(2,1)} %attend.1.flat_ref, bf16[512,1024]{1,0:T(8,128)(2,1)} %wo.1), custom_call_target="tpu_custom_call" | custom-call | tf_op jit(solution)/shard_map/mix/pallas_call | solution.py:459
  176.7 1.8 copy.56
  (2 shorter events, 0.0 us)
Async XLA Ops:
  5.4 106.5 %copy-start.2 = (f32[4]{0:T(128)S(1)}, f32[4]{0:T(128)}, u32[]{:S(2)}) copy-start(f32[4]{0:T(128)} %param.27) | copy-start | bytes 52
  5.4 106.5 %copy-start = (f32[48,4,4]{0,2,1:T(4,128)S(1)}, f32[48,4,4]{0,2,1:T(4,128)}, u32[]{:S(2)}) copy-start(f32[48,4,4]{0,2,1:T(4,128)} %param.29) | copy-start | bytes 9220
  5.4 106.5 %copy-start.1 = (f32[4]{0:T(128)S(1)}, f32[4]{0:T(128)}, u32[]{:S(2)}) copy-start(f32[4]{0:T(128)} %param.28) | copy-start | bytes 52

commit v4 on v3

--- a/solution.py
+++ b/solution.py
@@ -90,7 +90,9 @@
                 o_ref[seq, h] = c_scr[pl.ds(h * SB + seq, 1), :] * s_ref[seq, h] + add
 
 
-def attend_kernel(heads, s_ref, a_ref, q_ref, k_ref, v_ref, z_ref, d_ref, b_ref, w_ref, o_ref, rk, rq, qf, kf, vf, zf, of):
+def attend_kernel(heads, s_ref, a_ref, q_ref, k_ref, v_ref, z_ref, d_ref, b_ref, w_ref, o_ref, kept, rk, rq, qf, kf, vf, zf, of, done):
+    keep = pltpu.make_async_copy(s_ref, kept.at[pl.ds(pl.program_id(0) * SB, SB)], done)
+    keep.start()
     for src, dst in ((q_ref, qf), (k_ref, kf), (v_ref, vf), (z_ref, zf)):
         load_heads(heads, src, dst, a_ref[...])
     low = first_half()
@@ -130,6 +132,7 @@
             of[at, :] = att * lax.rsqrt(mean + epsilon) * gain * (gate * jax.nn.sigmoid(gate))
     for h in range(heads):
         o_ref[:, h * DK : (h + 1) * DK] = of[pl.ds(h * TALL, TALL), :].astype(bf16)
+    keep.wait()
 
 
 def accepted(state, keys, values, few):
@@ -165,9 +168,9 @@
         functools.partial(attend_kernel, heads),
         grid=(seqs // SB,),
         in_specs=[block, pl.BlockSpec((rows, 1), lambda i: (i, 0)), part(0), part(1), part(2), part(3), thin, thin, pl.BlockSpec((1, DK), lambda i: (0, 0))],
-        out_specs=pl.BlockSpec((rows, width), lambda i: (i, 0)),
-        out_shape=jax.ShapeDtypeStruct((seqs * P_SIZE, width), bf16),
-        scratch_shapes=[pltpu.VMEM((heads * TALL, DK), f32)] * 7,
+        out_specs=[pl.BlockSpec((rows, width), lambda i: (i, 0)), pl.BlockSpec(memory_space=pl.ANY)],
+        out_shape=[jax.ShapeDtypeStruct((seqs * P_SIZE, width), bf16), jax.ShapeDtypeStruct(state.shape, f32)],
+        scratch_shapes=[pltpu.VMEM((heads * TALL, DK), f32)] * 7 + [pltpu.SemaphoreType.DMA],
         cost_estimate=pl.CostEstimate(flops=5_000_000_000, bytes_accessed=state.size * 4, transcendentals=0),
         name="attend",
     )(state, factor, packed, packed, packed, packed, decay, beta, gain.reshape(1, DK))
@@ -187,8 +190,9 @@
 ORDER = ((3, 2, 1, 0), (0, 2, 1, 3), (3, 1, 2, 0), (0, 1, 2, 3))
 
 
-def project_kernel(x_ref, gain_ref, wq, wk, wv, wz, wf, ws, acc, few_ref, xbuf, w, fs, send, recv, esend, erecv,
-                   xs, xr, wsem, ps, pr, es, er):
+def project_kernel(x_ref, gain_ref, keys, values, thin, wq, wk, wv, wz, wf, ws, state, acc, few_ref, taken, xbuf, w, fs,
+                   send, recv, esend, erecv, s_in, s_out, r_scr, u_scr, c_scr, kf, vf,
+                   xs, xr, wsem, ps, pr, es, er, ins, outs):
     k, t, g = lax.axis_index("kv"), lax.axis_index("tp"), lax.axis_index("grp")
     depth, width = w.shape[1], w.shape[2]
     rows = x_ref.shape[0]
@@ -296,7 +300,41 @@
 
         return carry
 
-    lax.fori_loop(0, 4, step, 0)
+    lax.fori_loop(0, 3, step, 0)
+
+    blocks = state.shape[0] // SB
+    heads = state.shape[1]
+
+    def fetch(i):
+        return pltpu.make_async_copy(state.at[pl.ds(i * SB, SB)], s_in.at[i % 2], ins.at[i % 2])
+
+    def put(i):
+        return pltpu.make_async_copy(s_out.at[i % 2], taken.at[pl.ds(i * SB, SB)], outs.at[i % 2])
+
+    def accept(i, carry):
+        @pl.when(i + 1 < blocks)
+        def _():
+            fetch(i + 1).start()
+
+        fetch(i).wait()
+
+        @pl.when(i >= 2)
+        def _():
+            put(i - 2).wait()
+
+        tall, few_rows = pl.ds(i * TALL, TALL), pl.ds(i * SB, SB)
+        accepted_kernel(
+            heads, s_in.at[i % 2], keys.at[tall], values.at[tall], thin.at[few_rows], s_out.at[i % 2],
+            r_scr, u_scr, c_scr, kf, vf,
+        )
+        put(i).start()
+        return carry
+
+    fetch(0).start()
+    lax.fori_loop(0, blocks, accept, 0)
+    lax.fori_loop(3, 4, step, 0)
+    for i in range(max(blocks - 2, 0), blocks):
+        put(i).wait()
 
     first_wait = jnp.logical_not(home)
 
@@ -329,16 +367,21 @@
             lax.fori_loop(0, rows // 16, add, 0)
 
 
-def project(x, gain, weights, forgetting, strength):
+def project(x, gain, weights, forgetting, strength, state, keys, values, thin):
     rows, depth = x.shape
     width = weights[0].shape[1]
     vmem, hbm = pl.BlockSpec(memory_space=pltpu.VMEM), pl.BlockSpec(memory_space=pl.ANY)
     dma = pltpu.SemaphoreType.DMA
+    heads = state.shape[1]
     return pl.pallas_call(
         project_kernel,
-        in_specs=[vmem, vmem] + [hbm] * 6,
-        out_specs=[vmem, vmem],
-        out_shape=[jax.ShapeDtypeStruct((rows, 4 * width), f32), jax.ShapeDtypeStruct((40, rows), f32)],
+        in_specs=[vmem] * 5 + [hbm] * 7,
+        out_specs=[vmem, vmem, hbm],
+        out_shape=[
+            jax.ShapeDtypeStruct((rows, 4 * width), f32),
+            jax.ShapeDtypeStruct((40, rows), f32),
+            jax.ShapeDtypeStruct(state.shape, f32),
+        ],
         scratch_shapes=[
             pltpu.VMEM((4, rows, depth), bf16),
             pltpu.VMEM((4, depth, width), bf16),
@@ -347,11 +390,14 @@
             pltpu.VMEM((5, rows, 4 * width), bf16),
             pltpu.VMEM((4, 40, rows), f32),
             pltpu.VMEM((4, 40, rows), f32),
-            dma((4,)), dma((4,)), dma((6,)), dma((4,)), dma((5,)), dma((4,)), dma((4,)),
+            pltpu.VMEM((2, SB) + state.shape[1:], f32),
+            pltpu.VMEM((2, SB) + state.shape[1:], f32),
+            *[pltpu.VMEM((heads * n, DK), f32) for n in (TALL, TALL, SB, TALL, TALL)],
+            dma((4,)), dma((4,)), dma((6,)), dma((4,)), dma((5,)), dma((4,)), dma((4,)), dma((2,)), dma((2,)),
         ],
         compiler_params=pltpu.CompilerParams(has_side_effects=True, vmem_limit_bytes=56 * 2**20),
         name="project",
-    )(x, gain.reshape(-1, 1, depth), *weights, forgetting.T, strength.T)
+    )(x, gain.reshape(-1, 1, depth), keys, values, thin, *weights, forgetting.T, strength.T, state)
 
 
 NEAREST = ((0, 1, 2, 3), (1, 0, 2, 3), (2, 3, 1, 0), (3, 2, 1, 0))
@@ -509,9 +555,17 @@
         return values.reshape(seqs, P_SIZE * heads)
 
     weights = (probe_projector, address_projector, content_projector, sigmoid_mask_matrix)
+    earlier = (
+        memory_matrix,
+        earlier_addresses.reshape(rows, width),
+        earlier_contents.reshape(rows, width),
+        jnp.concatenate(
+            [thin(earlier_forgetting), thin(earlier_strengths), admitted_counts.astype(f32).reshape(seqs, 1)], axis=1
+        ),
+    )
     if n_kv == 4 and n_tp == 4:
-        summed, few = project(
-            candidate_embeddings, incoming_rms_scaling, weights, forgetting_projector, strength_projector_matrix
+        summed, few, taken = project(
+            candidate_embeddings, incoming_rms_scaling, weights, forgetting_projector, strength_projector_matrix, *earlier
         )
         columns = forgetting_projector.shape[1]
         few = [lax.dynamic_slice_in_dim(few, n * columns + t_index * heads, heads) for n in range(2)] + [few[2 * columns : 2 * columns + 1]]
@@ -536,20 +590,13 @@
             [jnp.dot(gained, w, preferred_element_type=f32).astype(bf16) for w in weights], axis=1
         )
         summed = lax.psum_scatter(partial, "kv", scatter_dimension=0, tiled=True).astype(f32)
-    taken = accepted(
-        memory_matrix,
-        earlier_addresses.reshape(rows, width),
-        earlier_contents.reshape(rows, width),
-        jnp.concatenate(
-            [thin(earlier_forgetting), thin(earlier_strengths), admitted_counts.astype(f32).reshape(seqs, 1)], axis=1
-        ),
-    )
+        taken = accepted(*earlier)
     factor = lax.rsqrt(few[:, 2 * heads :] / features + epsilon)
     few = few[:, : 2 * heads] * factor
     decay_in = few[:, :heads].reshape(seqs, P_SIZE, heads)
     beta = jax.nn.sigmoid(few[:, heads:].reshape(seqs, P_SIZE, heads))
     decay = -jnp.exp(channel_forgetting_rates) * jax.nn.softplus(decay_in + forgetting_offset) + extra_forgetting
-    flat = attend(taken, summed, factor, thin(decay), thin(beta), outgoing_rms_scaling)
+    flat, taken = attend(taken, summed, factor, thin(decay), thin(beta), outgoing_rms_scaling)
     if n_kv == 4 and n_tp == 4:
         mixed = mix(flat, final_projector)
     else:

time: 179 us -> 169 us (0.944)
  Pallas kernels: 167 us -> 156 us
    pallas_call x2 -> x1, Pallas kernels: 104 us -> 91.5 us  [project(): pl.pallas_call(project_kernel, in_specs=[vmem] * 5 + [hbm] * 7, out_specs...]
where the time goes in v4:
time: 169 us; the launch traced here: 168 us
  Pallas kernels  156 us (92%)
  local copies, waits for them, and re-layouts  8.22 us (5%)
  other arithmetic  3.04 us (2%)
    pallas_call x1, Pallas kernels, project(): pl.pallas_call(project_kernel, in_specs=[vmem] * 5 + [hbm] * 7, out_specs...  91.5 us
    pallas_call x1, Pallas kernels, mix(): pl.pallas_call(mix_kernel, in_specs=[vmem, hbm], out_specs=vmem, out_shap...  50.4 us
    pallas_call x1, Pallas kernels, attend(): pl.pallas_call(functools.partial(attend_kernel, heads), grid=(seqs // SB,...  14.3 us

profile of v4, /device:TPU:10, one launch (start us, length us, event | category | flops | bytes accessed | tf_op | source)
XLA Modules:
  0.0 168.1 jit_solution(3372160389569808868)
XLA Ops:
  0.6 0.0 copy-start
  0.6 0.0 copy-start.1
  0.7 0.7 exponential_negate_fusion
  1.3 0.7 convert_bitcast_fusion
  2.0 0.1 copy.45
  2.1 0.8 copy.44
  2.9 0.8 copy.43
  3.6 0.7 pad_maximum_fusion.thin
  4.3 1.8 %copy_bitcast_fusion = (bf16[192,512]{1,0:T(8,128)(2,1)}, bf16[192,512]{1,0:T(8,128)(2,1)}) fusion(bf16[24,8,4,128]{3,2,1,0:T(4,128)(2,1)} %bitcast.22, bf16[24,8,4,128]{3,2,1,0:T(4,128)(2,1)} %bitcast.23), kind=kLoop, calls=%fused_computation | loop fusion | bytes 786432 | tf_op jit(solution)/shard_map/reshape | solution.py:561
  6.1 91.5 %project.1 = (f32[192,2048]{1,0:T(8,128)}, f32[40,192]{1,0:T(8,128)}, f32[48,4,128,128]{3,2,1,0:T(8,128)}) custom-call(bf16[192,1024]{1,0:T(8,128)(2,1)} %x_ref.1, f32[4,1,1024]{2,1,0:T(1,128)} %bitcast.27, bf16[192,512]{1,0:T(8,128)(2,1)} %get-tuple-element.19.keys, bf16[192,512]{1,0:T(8,128)(2,1)} %get-tuple-element.18.values, ...), custom_call_target="tpu_custom_call" | custom-call | tf_op jit(solution)/shard_map/project/pallas_call | solution.py:376
  97.6 0.7 slice.15
  98.3 0.7 constant_dynamic-slice_fusion.1
  99.0 0.1 copy.46
  99.1 0.7 fusion.7
  99.9 0.1 slice_multiply_fusion
  100.0 0.1 fusion.2
  100.1 0.7 div.16.b_ref
  100.8 0.1 copy.47
  100.9 0.0 copy-done
  100.9 0.0 copy-done.1
  100.9 0.1 fusion.6
  101.0 0.7 copy.50.d_ref
  101.7 14.3 %attend.1 = (bf16[192,512]{1,0:T(8,128)(2,1)}, f32[48,4,128,128]{3,2,1,0:T(8,128)}) custom-call(f32[48,4,128,128]{3,2,1,0:T(8,128)} %get-tuple-element.7.s_ref, f32[192,1]{1,0:T(8,128)} %get-tuple-element.15.a_ref, f32[192,2048]{1,0:T(8,128)} %get-tuple-element.9.q_ref.k_ref.v_ref.z_ref, f32[192,2048]{1,0:T(8,128)} %get-tuple-element.9.q_ref.k_ref.v_ref.z_ref, ...), custom_call_target="tpu_custom_call" | custom-call | flops 5000000000 | bytes 12582912 | tf_op jit(solution)/shard_map/attend/pallas_call | solution.py:167
  115.9 50.4 %mix.1 = bf16[192,1024]{1,0:T(8,128)(2,1)} custom-call(bf16[192,512]{1,0:T(8,128)(2,1)} %get-tuple-element.10.flat_ref, bf16[512,1024]{1,0:T(8,128)(2,1)} %wo.1), custom_call_target="tpu_custom_call" | custom-call | tf_op jit(solution)/shard_map/mix/pallas_call | solution.py:505
  166.3 1.8 %copy.56 = bf16[192,1024]{1,0:T(8,128)(2,1)} copy(bf16[192,1024]{1,0:T(8,128)(2,1)} %mix.1) | data formatting | bytes 786432
  (1 shorter events, 0.0 us)
Async XLA Ops:
  0.6 100.3 %copy-start = (f32[48,4,4]{0,2,1:T(4,128)S(1)}, f32[48,4,4]{0,2,1:T(4,128)}, u32[]{:S(2)}) copy-start(f32[48,4,4]{0,2,1:T(4,128)} %param.29) | copy-start | bytes 9220
  0.6 100.2 %copy-start.1 = (f32[4]{0:T(128)S(1)}, f32[4]{0:T(128)}, u32[]{:S(2)}) copy-start(f32[4]{0:T(128)} %param.28) | copy-start | bytes 52

commit v5 on v4

--- a/solution.py
+++ b/solution.py
@@ -241,17 +241,7 @@
     over.start()
     near = remote(xbuf.at[slot], xbuf.at[slot], xs.at[2], xr.at[slot], k, beside)
     near.start()
-    other = turned_slot(across)
-    arrived(other)
-    onward = remote(xbuf.at[other], xbuf.at[other], xs.at[3], xr.at[other], k, beside)
-    onward.start()
-    arrived(turned_slot(beside))
-    arrived(turned_slot((beside + 2) % 4))
-    for load in loads:
-        load.wait()
-
-    def step(i, carry):
-        r = pick(k, [pick(i, row) for row in ORDER])
+    def block(r):
         own = r == k
         floated = xbuf[r].astype(f32)
         gained = (floated * gain_ref[k]).astype(bf16)
@@ -297,6 +287,29 @@
             place = jnp.where(ends, 4, k)
             remote(send.at[r], recv.at[place], ps.at[r], pr.at[place], target, t).start()
             remote(esend.at[r], erecv.at[k], es.at[r], er.at[k], r, t).start()
+
+    for load in loads:
+        load.wait()
+    held_back = jnp.logical_or(jnp.logical_and(k == 1, slot == 3), jnp.logical_and(k == 2, slot == 0))
+    early = jnp.logical_and(slot != k, jnp.logical_not(held_back))
+
+    @pl.when(early)
+    def _():
+        block(slot)
+
+    other = turned_slot(across)
+    arrived(other)
+    onward = remote(xbuf.at[other], xbuf.at[other], xs.at[3], xr.at[other], k, beside)
+    onward.start()
+    arrived(turned_slot(beside))
+    arrived(turned_slot((beside + 2) % 4))
+
+    def step(i, carry):
+        r = pick(k, [pick(i, row) for row in ORDER])
+
+        @pl.when(jnp.logical_not(jnp.logical_and(early, r == slot)))
+        def _():
+            block(r)
 
         return carry
 

time: 169 us -> 169 us (level)
  no operation moved by 1% of the time
where the time goes in v5:
time: 169 us; the launch traced here: 168 us
  Pallas kernels  156 us (92%)
  local copies, waits for them, and re-layouts  8.22 us (5%)
  other arithmetic  3.04 us (2%)
    pallas_call x1, Pallas kernels, project(): pl.pallas_call(project_kernel, in_specs=[vmem] * 5 + [hbm] * 7, out_specs...  91.8 us
    pallas_call x1, Pallas kernels, mix(): pl.pallas_call(mix_kernel, in_specs=[vmem, hbm], out_specs=vmem, out_shap...  50.4 us
    pallas_call x1, Pallas kernels, attend(): pl.pallas_call(functools.partial(attend_kernel, heads), grid=(seqs // SB,...  14.3 us

profile of v5, /device:TPU:10, one launch (start us, length us, event | category | flops | bytes accessed | tf_op | source)
XLA Modules:
  0.0 168.4 jit_solution(16548029936033148224)
XLA Ops:
  0.6 0.0 copy-start
  0.6 0.0 copy-start.1
  0.7 0.7 exponential_negate_fusion
  1.3 0.7 convert_bitcast_fusion
  2.0 0.1 copy.45
  2.1 0.8 copy.44
  2.9 0.8 copy.43
  3.6 0.7 pad_maximum_fusion.thin
  4.3 1.8 %copy_bitcast_fusion = (bf16[192,512]{1,0:T(8,128)(2,1)}, bf16[192,512]{1,0:T(8,128)(2,1)}) fusion(bf16[24,8,4,128]{3,2,1,0:T(4,128)(2,1)} %bitcast.22, bf16[24,8,4,128]{3,2,1,0:T(4,128)(2,1)} %bitcast.23), kind=kLoop, calls=%fused_computation | loop fusion | bytes 786432 | tf_op jit(solution)/shard_map/reshape | solution.py:574
  6.1 91.8 %project.1 = (f32[192,2048]{1,0:T(8,128)}, f32[40,192]{1,0:T(8,128)}, f32[48,4,128,128]{3,2,1,0:T(8,128)}) custom-call(bf16[192,1024]{1,0:T(8,128)(2,1)} %x_ref.1, f32[4,1,1024]{2,1,0:T(1,128)} %bitcast.27, bf16[192,512]{1,0:T(8,128)(2,1)} %get-tuple-element.19.keys, bf16[192,512]{1,0:T(8,128)(2,1)} %get-tuple-element.18.values, ...), custom_call_target="tpu_custom_call" | custom-call | tf_op jit(solution)/shard_map/project/pallas_call | solution.py:389
  97.9 0.7 slice.15
  98.6 0.7 constant_dynamic-slice_fusion.1
  99.3 0.1 copy.46
  99.4 0.7 fusion.7
  100.2 0.1 slice_multiply_fusion
  100.3 0.1 fusion.2
  100.4 0.7 div.16.b_ref
  101.1 0.1 copy.47
  101.2 0.0 copy-done
  101.2 0.0 copy-done.1
  101.2 0.1 fusion.6
  101.3 0.7 copy.50.d_ref
  102.0 14.3 %attend.1 = (bf16[192,512]{1,0:T(8,128)(2,1)}, f32[48,4,128,128]{3,2,1,0:T(8,128)}) custom-call(f32[48,4,128,128]{3,2,1,0:T(8,128)} %get-tuple-element.7.s_ref, f32[192,1]{1,0:T(8,128)} %get-tuple-element.15.a_ref, f32[192,2048]{1,0:T(8,128)} %get-tuple-element.9.q_ref.k_ref.v_ref.z_ref, f32[192,2048]{1,0:T(8,128)} %get-tuple-element.9.q_ref.k_ref.v_ref.z_ref, ...), custom_call_target="tpu_custom_call" | custom-call | flops 5000000000 | bytes 12582912 | tf_op jit(solution)/shard_map/attend/pallas_call | solution.py:167
  116.2 50.4 %mix.1 = bf16[192,1024]{1,0:T(8,128)(2,1)} custom-call(bf16[192,512]{1,0:T(8,128)(2,1)} %get-tuple-element.10.flat_ref, bf16[512,1024]{1,0:T(8,128)(2,1)} %wo.1), custom_call_target="tpu_custom_call" | custom-call | tf_op jit(solution)/shard_map/mix/pallas_call | solution.py:518
  166.6 1.8 %copy.56 = bf16[192,1024]{1,0:T(8,128)(2,1)} copy(bf16[192,1024]{1,0:T(8,128)(2,1)} %mix.1) | data formatting | bytes 786432
  (1 shorter events, 0.0 us)
Async XLA Ops:
  0.6 100.5 %copy-start = (f32[48,4,4]{0,2,1:T(4,128)S(1)}, f32[48,4,4]{0,2,1:T(4,128)}, u32[]{:S(2)}) copy-start(f32[48,4,4]{0,2,1:T(4,128)} %param.29) | copy-start | bytes 9220
  0.6 100.5 %copy-start.1 = (f32[4]{0:T(128)S(1)}, f32[4]{0:T(128)}, u32[]{:S(2)}) copy-start(f32[4]{0:T(128)} %param.28) | copy-start | bytes 52
